TPU v7x, 32 devices: a whole 2x2x4 slice. The times are simulated.
32 devices in a mesh: sp: 8 (over z, y), tp: 4 (over x, core).
Axes of the slice: x: 2, y: 2, z: 4, core: 2. Of those that a mesh axis runs over, the one named last changes fastest.
Arguments:
- tokens: bfloat16 [4096, 2048], P('sp', 'tp'), may hold values from -6 to 6
- norm_gain: float32 [2048], replicated, may hold values from 0.1 to 1.9
- query_weight: bfloat16 [2048, 2048], P('sp', 'tp'), may hold values from -0.125 to 0.125
- key_weight: bfloat16 [2048, 512], P('sp', 'tp'), may hold values from -0.125 to 0.125
- value_weight: bfloat16 [2048, 512], P('sp', 'tp'), may hold values from -0.125 to 0.125
- pool_in_weight: bfloat16 [2048, 1024], P('sp', 'tp'), may hold values from -0.125 to 0.125
- pool_mix_weight: bfloat16 [4, 256, 256], P('tp'), may hold values from -0.375 to 0.375
- sink_logit: float32 [32], P('tp'), may hold values from -300 to 300
- out_pool_weight: bfloat16 [1024, 2048], P('tp', 'sp'), may hold values from -0.109375 to 0.109375
- out_attn_weight: bfloat16 [2048, 2048], P('tp', 'sp'), may hold values from -1.25 to 1.25
Outputs:
- mixed: bfloat16 [4096, 2048], P('sp', 'tp')
- log_weight: float32 [32, 4096], P('tp', 'sp')
All inputs are finite; a program needn't handle non-finite values.
Results may differ from a plain program's by a relative error of at most 0.012.
Values may be sent and summed in bfloat16 or wider, within the bound.
A program may use at most 64 MiB of HBM per device.

v0:
```python
import functools
import math

import jax
import jax.numpy as jnp
from jax import lax
from jax.experimental import pallas as pl
from jax.experimental.pallas import tpu as pltpu
from jax.sharding import PartitionSpec as P

HD = 64
WINDOW = 128
GRID_W = 64


norm_eps = 1e-06
rope_base = 10000.0
pool_reach = 8
neg_fill = -1e30


def with_halo(cells, sides, width):
    for axis, dim in sides:
        count = lax.axis_size(axis)
        ends = count - 1
        head = lax.slice_in_dim(cells, 0, width, axis=dim)
        tail = lax.slice_in_dim(cells, cells.shape[dim] - width, cells.shape[dim], axis=dim)
        cells = jnp.concatenate(
            [
                lax.ppermute(tail, axis, [(i, (i + 1) % count) for i in range(ends)]),
                cells,
                lax.ppermute(head, axis, [((i + 1) % count, i) for i in range(ends)]),
            ],
            axis=dim,
        )
    return cells


def rope_tables(positions, head_dim):
    n_freq = head_dim // 4
    freqs = rope_base ** (-jnp.arange(n_freq, dtype=jnp.float32) / n_freq)
    rows = (positions // GRID_W).astype(jnp.float32)
    columns = (positions % GRID_W).astype(jnp.float32)
    row_angle = rows[:, None] * freqs[None, :]
    col_angle = columns[:, None] * freqs[None, :]
    return (jnp.cos(row_angle), jnp.sin(row_angle), jnp.cos(col_angle), jnp.sin(col_angle))


def rotate_half(values, cosine, sine):
    middle = values.shape[-1] // 2
    first = values[..., :middle]
    second = values[..., middle:]
    return jnp.concatenate([first * cosine - second * sine, second * cosine + first * sine], -1)


def rotate_heads(values, tables, head_dim):
    rows_count = values.shape[0]
    shaped = values.astype(jnp.float32).reshape(rows_count, -1, head_dim)
    cos_r, sin_r, cos_c, sin_c = [table[:, None, :] for table in tables]
    split = head_dim // 2
    turned = jnp.concatenate(
        [
            rotate_half(shaped[..., :split], cos_r, sin_r),
            rotate_half(shaped[..., split:], cos_c, sin_c),
        ],
        -1,
    )
    return turned.reshape(rows_count, -1).astype(jnp.bfloat16)


def pool_group(extended, own, positions, half_width, seq_total):
    rows_count = own.shape[0]
    summed = jnp.zeros(own.shape, jnp.float32)
    counted = jnp.zeros((rows_count,), jnp.float32)
    for shift_by in range(-pool_reach, pool_reach):
        source = positions + shift_by
        inside = (
            (shift_by >= -half_width)
            & (shift_by < half_width)
            & (source >= 0)
            & (source < seq_total)
        )
        window_rows = extended[pool_reach + shift_by : pool_reach + shift_by + rows_count].astype(
            jnp.float32
        )
        summed = summed + jnp.where(inside[:, None], window_rows, 0.0)
        counted = counted + inside.astype(jnp.float32)
    return (summed / counted[:, None] - own.astype(jnp.float32)).astype(jnp.bfloat16)


def attend_block(queries, keys, values, sink, query_pos, key_pos, seq_total):
    scores = jnp.einsum(
        "qhgd,khd->hgqk", queries, keys, preferred_element_type=jnp.float32
    ) * HD ** (-0.5)
    valid = (
        (jnp.abs(query_pos[:, None] - key_pos[None, :]) <= WINDOW)
        & (key_pos >= 0)[None, :]
        & (key_pos < seq_total)[None, :]
    )
    scores = jnp.where(valid, scores, neg_fill)
    row_top = jnp.maximum(jnp.max(scores, -1), sink[:, :, None])
    exps = jnp.exp(scores - row_top[..., None])
    row_total = jnp.sum(exps, -1) + jnp.exp(sink[:, :, None] - row_top)
    weights = (exps / row_total[..., None]).astype(jnp.bfloat16)
    attended = jnp.einsum("hgqk,khd->qhgd", weights, values, preferred_element_type=jnp.float32)
    return (attended.astype(jnp.bfloat16), row_top + jnp.log(row_total))


def fetch_outputs(out_pool_weight, out_attn_weight):
    return (
        lax.all_gather(out_pool_weight, "sp", axis=1, tiled=True),
        lax.all_gather(out_attn_weight, "sp", axis=1, tiled=True),
    )


def local(
    tokens,
    norm_gain,
    query_weight,
    key_weight,
    value_weight,
    pool_in_weight,
    pool_mix_weight,
    sink_logit,
    out_pool_weight,
    out_attn_weight,
):
    whole = lax.all_gather(tokens, "tp", axis=1, tiled=True)
    wide = whole.astype(jnp.float32)
    normed = (
        wide * lax.rsqrt(jnp.mean(wide * wide, -1, keepdims=True) + norm_eps) * norm_gain
    ).astype(jnp.bfloat16)
    tok_rows = normed.shape[0]
    seq_total = tok_rows * lax.axis_size("sp")
    offset = lax.axis_index("sp") * tok_rows
    weights_in = (query_weight, key_weight, value_weight, pool_in_weight)
    pieces = (
        lax.all_gather(weights_in[0], "sp", axis=0, tiled=True),
        lax.all_gather(weights_in[1], "sp", axis=0, tiled=True),
        lax.all_gather(weights_in[2], "sp", axis=0, tiled=True),
        lax.all_gather(weights_in[3], "sp", axis=0, tiled=True),
    )
    sums = tuple((jnp.dot(normed, piece, preferred_element_type=jnp.float32) for piece in pieces))
    query, key, value, pool_input = [total.astype(jnp.bfloat16) for total in sums]
    positions = offset + jnp.arange(tok_rows, dtype=jnp.int32)
    tables = rope_tables(positions, HD)
    rot_query = rotate_heads(query, tables, HD)
    rot_key = rotate_heads(key, tables, HD)
    key_width = rot_key.shape[1]
    pool_ext = with_halo(pool_input, (("sp", 0),), pool_reach)
    pair_ext = with_halo(jnp.concatenate([rot_key, value], 1), (("sp", 0),), WINDOW)
    key_ext = pair_ext[:, :key_width]
    value_ext = pair_ext[:, key_width:]
    half_width = jnp.left_shift(jnp.int32(1), lax.axis_index("tp"))
    pooled = pool_group(pool_ext, pool_input, positions, half_width, seq_total)
    pool_out = jnp.dot(pooled, pool_mix_weight[0], preferred_element_type=jnp.float32).astype(
        jnp.bfloat16
    )
    heads_local = rot_query.shape[1] // HD
    kv_local = key_width // HD
    grp = heads_local // kv_local
    query_heads = rot_query.reshape(tok_rows, kv_local, grp, HD)
    key_heads = key_ext.reshape(-1, kv_local, HD)
    value_heads = value_ext.reshape(-1, kv_local, HD)
    sink = sink_logit.reshape(kv_local, grp)
    block_rows = min(tok_rows, 256)
    attended_parts = []
    log_parts = []
    for block_index in range(tok_rows // block_rows):
        start = block_index * block_rows
        query_pos = offset + start + jnp.arange(block_rows, dtype=jnp.int32)
        key_pos = offset + start - WINDOW + jnp.arange(block_rows + 2 * WINDOW, dtype=jnp.int32)
        attended_block, log_block = attend_block(
            query_heads[start : start + block_rows],
            key_heads[start : start + block_rows + 2 * WINDOW],
            value_heads[start : start + block_rows + 2 * WINDOW],
            sink,
            query_pos,
            key_pos,
            seq_total,
        )
        attended_parts.append(attended_block.reshape(block_rows, heads_local * HD))
        log_parts.append(log_block.reshape(heads_local, block_rows))
    attended = jnp.concatenate(attended_parts, 0)
    log_weight = jnp.concatenate(log_parts, 1)
    out_pool_full, out_attn_full = fetch_outputs(out_pool_weight, out_attn_weight)
    term = jnp.dot(pool_out, out_pool_full, preferred_element_type=jnp.float32)
    term = term + jnp.dot(attended, out_attn_full, preferred_element_type=jnp.float32)
    mixed = lax.psum_scatter(term.astype(jnp.bfloat16), "tp", scatter_dimension=1, tiled=True)
    return (mixed, log_weight)


NY = 2
PIECES = 4
MESH = pl.DeviceIdType.MESH


def layer_kernel(
    nz,
    ntp,
    tok_ref,
    gain_ref,
    qw_ref,
    kw_ref,
    vw_ref,
    pw_ref,
    mix_ref,
    sink_ref,
    ow_ref,
    aw_ref,
    mixed_ref,
    log_ref,
    xg,
    normed,
    wg,
    wo,
    qrot,
    ext,
    act,
    part,
    rsb,
    cos_ref,
    sin_ref,
    pair,
    total_out,
    loc_sem,
    w_send,
    w_recv,
    x_send,
    x_recv,
    h_send,
    h_recv,
    r_send,
    r_recv,
    p_send,
    p_recv,
):
    sp, tp = lax.axis_index("sp"), lax.axis_index("tp")
    nsp = nz * NY
    z, y = sp // NY, sp % NY
    rows = tok_ref.shape[0]
    width = tok_ref.shape[1]
    brow = qw_ref.shape[0]
    qn, kn, pn = qw_ref.shape[1], kw_ref.shape[1], pw_ref.shape[1]
    pool_rows = ow_ref.shape[0]
    fan = wo.shape[1]
    ocols = wo.shape[2]
    seq_total = rows * nsp
    heads, kv_local = qn // HD, kn // HD
    grp = heads // kv_local

    base = pl.multiple_of(sp * brow, brow)
    own = [
        (tok_ref, xg.at[tp]),
        (qw_ref, wg.at[pl.ds(base, brow), pl.ds(0, qn)]),
        (kw_ref, wg.at[pl.ds(base, brow), pl.ds(qn, kn)]),
        (vw_ref, wg.at[pl.ds(base, brow), pl.ds(qn + kn, kn)]),
        (pw_ref, wg.at[pl.ds(base, brow), pl.ds(qn + 2 * kn, pn)]),
        (ow_ref, wo.at[sp, pl.ds(0, pool_rows)]),
        (aw_ref, wo.at[sp, pl.ds(pool_rows, fan - pool_rows)]),
    ]
    local_copies = [pltpu.make_async_copy(a, b, loc_sem.at[i]) for i, (a, b) in enumerate(own)]
    for copy in local_copies:
        copy.start()
    ext[...] = jnp.zeros_like(ext)

    barrier = pltpu.get_barrier_semaphore()
    sp_peers = [
        (z + 1 < nz, sp + NY),
        (z >= 1, sp - NY),
        (z >= 0, z * NY + (1 - y)),
        (sp + 1 < nsp, sp + 1),
        (sp >= 1, sp - 1),
    ]
    expected = ntp - 1
    for ok, peer in sp_peers:
        expected = expected + ok.astype(jnp.int32)

        @pl.when(ok)
        def _():
            pl.semaphore_signal(barrier, inc=1, device_id={"sp": peer}, device_id_type=MESH)

    for step in range(1, ntp):
        other = lax.rem(tp + step, ntp)
        pl.semaphore_signal(barrier, inc=1, device_id={"tp": other}, device_id_type=MESH)
    for copy in local_copies:
        copy.wait()
    pl.semaphore_wait(barrier, expected)

    def weight_copy(kind, block, piece, way):
        if kind == 0:
            size = brow // PIECES
            start = pl.multiple_of(block * brow + piece * size, size)
            ref = wg.at[pl.ds(start, size)]
        else:
            size = fan // PIECES
            ref = wo.at[block, pl.ds(piece * size, size)]
        target = (sp + NY, sp - NY, z * NY + (1 - y))[way]
        return pltpu.make_async_remote_copy(
            src_ref=ref,
            dst_ref=ref,
            send_sem=w_send.at[kind, way, block, piece],
            recv_sem=w_recv.at[kind, block, piece],
            device_id={"sp": target},
            device_id_type=MESH,
        )

    onward = (z + 1 < nz, z >= 1)

    def issue(copy, done):
        if done:
            copy.wait_send()
        else:
            copy.start()

    last = PIECES - 1

    def relay(kind, d, done=False):
        for piece in range(PIECES):
            for way in range(2):
                source = (z - d, z + d)[way]
                block = source * NY + y
                valid = (source >= 0) & (source < nz)

                @pl.when(valid)
                def _():
                    if not done:
                        weight_copy(kind, block, piece, 2).wait_recv()

                    @pl.when(onward[way])
                    def _():
                        issue(weight_copy(kind, block, piece, way), done)

                    if kind == 1 or piece != last:
                        issue(weight_copy(kind, block, piece, 2), done)

    def own_row(kind, way, done=False):
        for piece in range(PIECES):
            if way == 2:
                issue(weight_copy(kind, sp, piece, way), done)
            else:

                @pl.when(onward[way])
                def _():
                    issue(weight_copy(kind, sp, piece, way), done)

    def relay_other(d, done=False):
        if d == 0:
            block = z * NY + (1 - y)
            if not done:
                weight_copy(0, block, last, 2).wait_recv()
            for way in range(2):

                @pl.when(onward[way])
                def _():
                    issue(weight_copy(0, block, last, way), done)

        else:
            for way in range(2):
                source = (z - d, z + d)[way]

                @pl.when((source >= 0) & (source < nz))
                def _():
                    block = source * NY + (1 - y)
                    if not done:
                        weight_copy(0, block, last, 2).wait_recv()

                    @pl.when(onward[way])
                    def _():
                        issue(weight_copy(0, block, last, way), done)

    def token_copy(step):
        other = lax.rem(tp + step, ntp)
        return pltpu.make_async_remote_copy(
            src_ref=xg.at[tp],
            dst_ref=xg.at[tp],
            send_sem=x_send.at[step],
            recv_sem=x_recv.at[tp],
            device_id={"tp": other},
            device_id_type=MESH,
        )

    def token_wait(step):
        other = lax.rem(tp + step, ntp)
        return pltpu.make_async_remote_copy(
            src_ref=xg.at[other],
            dst_ref=xg.at[other],
            send_sem=x_send.at[step],
            recv_sem=x_recv.at[other],
            device_id={"tp": other},
            device_id_type=MESH,
        )

    for piece in range(PIECES):
        for way in range(2):

            @pl.when(onward[way])
            def _():
                weight_copy(0, sp, piece, way).start()

        weight_copy(0, sp, piece, 2).start()
    for step in range(1, ntp):
        token_copy(step).start()

    def out_starts(d):
        @pl.when(z == d)
        def _():
            own_row(1, 0)

        @pl.when(nz - 1 - z == d)
        def _():
            own_row(1, 1)

    half = HD // 4
    lane = lax.broadcasted_iota(jnp.int32, (rows, 128), 1)
    is_first = (lane % (2 * half)) < half
    position = sp * rows + lax.broadcasted_iota(jnp.int32, (rows, 128), 0)
    place = jnp.where((lane % HD) < 2 * half, position // GRID_W, position % GRID_W)
    freqs = jnp.exp((lane % half).astype(jnp.float32) * (-math.log(rope_base) / half))
    angle = place.astype(jnp.float32) * freqs
    cos_ref[...] = jnp.cos(angle)
    sine = jnp.sin(angle)
    sin_ref[...] = jnp.where(is_first, -sine, sine)

    for d in range(1, nz - 1):
        relay(0, d)
        relay_other(d - 1)
        out_starts(d - 1)
    own_row(1, 2)

    for step in range(1, ntp):
        token_wait(step).wait_recv()

    norm_rows = 64

    @pl.loop(0, rows // norm_rows)
    def _(i):
        at = pl.ds(pl.multiple_of(i * norm_rows, norm_rows), norm_rows)
        pieces = [xg[t, at, :].astype(jnp.float32) for t in range(ntp)]
        total = sum(jnp.sum(piece * piece, -1, keepdims=True) for piece in pieces)
        scale = lax.rsqrt(total / (width * ntp) + norm_eps)
        for t in range(ntp):
            cols = pl.ds(t * width, width)
            normed[at, cols] = (pieces[t] * scale * gain_ref[:, cols]).astype(jnp.bfloat16)

    for d in range(max(nz - 1, 1), nz):
        relay(0, d)
    for d in range(max(nz - 2, 0), nz):
        relay_other(d)
        out_starts(d)

    for source in range(nz):
        for piece in range(PIECES - 1):
            weight_copy(0, source * NY + (1 - y), piece, 2).wait_recv()

    def turn(values, factor):
        wide = values.astype(jnp.bfloat16).astype(jnp.float32)
        swapped = jnp.where(
            is_first, pltpu.roll(wide, 128 - half, 1), pltpu.roll(wide, half, 1)
        )
        return ((wide * cos_ref[...] + swapped * sin_ref[...]) * factor).astype(jnp.bfloat16)

    def project(start, size):
        return jnp.dot(normed[...], wg[:, start : start + size], preferred_element_type=jnp.float32)

    mid = pl.ds(WINDOW, rows)
    for c in range(0, kn, 128):
        ext[mid, c : c + 128] = turn(project(qn + c, 128), 1.0)
    ext[mid, kn : 2 * kn] = project(qn + kn, kn).astype(jnp.bfloat16)
    ext[mid, 2 * kn : 2 * kn + pn] = project(qn + 2 * kn, pn).astype(jnp.bfloat16)
    for c in range(0, qn, 256):
        both = project(qn * 0 + c, 256)
        qrot[:, c : c + 128] = turn(both[:, :128], HD ** -0.5)
        qrot[:, c + 128 : c + 256] = turn(both[:, 128:], HD ** -0.5)

    edge = 16

    def halo_copy(way, what):
        cols = pl.ds(0, 2 * kn) if what == 0 else pl.ds(2 * kn, pn)
        count = WINDOW if what == 0 else edge
        if way == 0:
            src, dst = WINDOW + rows - count, WINDOW - count
            target = sp + 1
        else:
            src, dst = WINDOW, WINDOW + rows
            target = sp - 1
        return pltpu.make_async_remote_copy(
            src_ref=ext.at[pl.ds(src, count), cols],
            dst_ref=ext.at[pl.ds(dst, count), cols],
            send_sem=h_send.at[way, what],
            recv_sem=h_recv.at[way, what],
            device_id={"sp": target},
            device_id_type=MESH,
        )

    has_next, has_prev = sp + 1 < nsp, sp >= 1

    for way, ok in ((0, has_next), (1, has_prev)):
        @pl.when(ok)
        def _():
            halo_copy(way, 0).start()
            halo_copy(way, 1).start()

    for d in range(1, min(nz, 2)):
        relay(1, d)

    span = 3 * WINDOW
    row_at = lax.broadcasted_iota(jnp.int32, (WINDOW, span), 0)
    key_at = lax.broadcasted_iota(jnp.int32, (WINDOW, span), 1)
    half_width = jnp.left_shift(jnp.int32(1), tp)

    def mixer_block(i):
        q_at = slice(i * WINDOW, (i + 1) * WINDOW)
        window = slice(i * WINDOW, i * WINDOW + span)
        first = sp * rows + (i - 1) * WINDOW
        inside = (key_at + first >= 0) & (key_at + first < seq_total)
        apart = key_at - row_at
        band = inside & (apart >= WINDOW - half_width) & (apart < WINDOW + half_width)
        band_f = band.astype(jnp.float32)
        counted = jnp.sum(band_f, -1, keepdims=True)
        summed = jnp.dot(
            band_f.astype(jnp.bfloat16),
            ext[window, 2 * kn : 2 * kn + pn],
            preferred_element_type=jnp.float32,
        )
        own_pool = ext[(i + 1) * WINDOW : (i + 2) * WINDOW, 2 * kn : 2 * kn + pn]
        pooled = (summed / counted - own_pool.astype(jnp.float32)).astype(jnp.bfloat16)
        act[q_at, 0:pn] = jnp.dot(
            pooled, mix_ref[0], preferred_element_type=jnp.float32
        ).astype(jnp.bfloat16)
        valid = inside & (apart >= 0) & (apart <= 2 * WINDOW)
        logs = jnp.zeros((WINDOW, 128), jnp.float32)
        lane_at = lax.broadcasted_iota(jnp.int32, (WINDOW, 128), 1)
        for kv in range(kv_local):
            keys = ext[window, kv * HD : (kv + 1) * HD]
            values = ext[window, kn + kv * HD : kn + (kv + 1) * HD]
            outs = []
            for g in range(grp):
                head = kv * grp + g
                query = qrot[q_at, head * HD : (head + 1) * HD]
                score = lax.dot_general(
                    query, keys, (((1,), (1,)), ((), ())), preferred_element_type=jnp.float32
                )
                score = jnp.where(valid, score, neg_fill)
                sink = sink_ref[head]
                top = jnp.maximum(jnp.max(score, -1, keepdims=True), sink)
                exps = jnp.exp(score - top)
                total = jnp.sum(exps, -1, keepdims=True) + jnp.exp(sink - top)
                weights = (exps * (1.0 / total)).astype(jnp.bfloat16)
                outs.append(jnp.dot(weights, values, preferred_element_type=jnp.float32))
                logs = jnp.where(lane_at == head, top + jnp.log(total), logs)
            for g in range(0, grp, 2):
                at = pn + (kv * grp + g) * HD
                act[q_at, at : at + 2 * HD] = jnp.concatenate(outs[g : g + 2], 1).astype(
                    jnp.bfloat16
                )
        log_ref[:, q_at] = logs.T[:heads, :]

    n_blocks = rows // WINDOW
    for i in range(1, n_blocks - 1):
        mixer_block(i)
    for d in range(2, min(nz, 3)):
        relay(1, d)
    for way, ok in ((0, has_prev), (1, has_next)):
        @pl.when(ok)
        def _():
            halo_copy(way, 0).wait_recv()
            halo_copy(way, 1).wait_recv()

    for i in (0, n_blocks - 1):
        mixer_block(i)

    per_owner = nsp // ntp

    mate = tp + 1 - 2 * (tp % 2)

    def on_chip(block):
        return (block // per_owner) // 2 == tp // 2

    def is_mine(block):
        return block // per_owner == tp

    def is_joined(block):
        return jnp.logical_not(on_chip(block)) & ((block // per_owner) % 2 == tp % 2)

    def is_lent(block):
        return jnp.logical_not(on_chip(block)) & ((block // per_owner) % 2 != tp % 2)

    def reduce_copy(block, source):
        slot = block % per_owner
        return pltpu.make_async_remote_copy(
            src_ref=source.at[block],
            dst_ref=rsb.at[tp, slot],
            send_sem=r_send.at[block],
            recv_sem=r_recv.at[tp, slot],
            device_id={"tp": block // per_owner},
            device_id_type=MESH,
        )

    def lend_copy(block):
        return pltpu.make_async_remote_copy(
            src_ref=part.at[block],
            dst_ref=pair.at[block],
            send_sem=p_send.at[block],
            recv_sem=p_recv.at[block],
            device_id={"tp": mate},
            device_id_type=MESH,
        )

    def out_block(block):
        part[block] = jnp.dot(act[...], wo[block], preferred_element_type=jnp.float32).astype(
            jnp.bfloat16
        )

        @pl.when(on_chip(block) & jnp.logical_not(is_mine(block)))
        def _():
            reduce_copy(block, part).start()

        @pl.when(is_lent(block))
        def _():
            lend_copy(block).start()

    def join_block(block):
        @pl.when(is_joined(block))
        def _():
            lend_copy(block).wait_recv()
            total_out[block] = (
                part[block].astype(jnp.float32) + pair[block].astype(jnp.float32)
            ).astype(jnp.bfloat16)
            reduce_copy(block, total_out).start()

    def row_steps(low, high):
        @pl.loop(2 * low, 2 * high)
        def _(k):
            d = k // 2
            source = z + (2 * (k % 2) - 1) * d

            @pl.when((source >= 0) & (source < nz) & ((d > 0) | (k % 2 == 0)))
            def _():
                out_block(source * NY + y)
                join_block(source * NY + y)

    def other_steps(low, high):
        @pl.loop(2 * low, 2 * high)
        def _(k):
            d = k // 2
            source = z + (2 * (k % 2) - 1) * d

            @pl.when((source >= 0) & (source < nz) & ((d > 0) | (k % 2 == 0)))
            def _():
                block = source * NY + (1 - y)
                for piece in range(PIECES):
                    weight_copy(1, block, piece, 2).wait_recv()
                out_block(block)
                join_block(block)

    near = min(nz, 3)
    row_steps(0, near)
    other_steps(0, min(nz, 2))
    for d in range(3, nz):
        relay(1, d)
    row_steps(near, nz)
    other_steps(min(nz, 2), nz)

    for slot in range(per_owner):
        total = part[tp * per_owner + slot].astype(jnp.float32)
        for step in range(ntp // 2):
            other = mate if step == 0 else lax.rem(tp + 2 * step, ntp)
            pltpu.make_async_remote_copy(
                src_ref=rsb.at[other, slot],
                dst_ref=rsb.at[other, slot],
                send_sem=r_send.at[slot],
                recv_sem=r_recv.at[other, slot],
                device_id={"tp": other},
                device_id_type=MESH,
            ).wait_recv()
            total = total + rsb[other, slot].astype(jnp.float32)
        mixed_ref[:, slot * ocols : (slot + 1) * ocols] = total.astype(jnp.bfloat16)

    for step in range(1, ntp):
        token_copy(step).wait_send()
    for kind in range(2):
        for way in range(3):
            own_row(kind, way, done=True)
        for d in range(1, nz):
            relay(kind, d, done=True)
    for d in range(nz):
        relay_other(d, done=True)
    for way, ok in ((0, has_next), (1, has_prev)):
        @pl.when(ok)
        def _():
            halo_copy(way, 0).wait_send()
            halo_copy(way, 1).wait_send()

    @pl.loop(0, nsp)
    def _(block):
        @pl.when((on_chip(block) & jnp.logical_not(is_mine(block))) | is_joined(block))
        def _():
            reduce_copy(block, part).wait_send()

        @pl.when(is_lent(block))
        def _():
            lend_copy(block).wait_send()


def fused(
    nz,
    ntp,
    tokens,
    norm_gain,
    query_weight,
    key_weight,
    value_weight,
    pool_in_weight,
    pool_mix_weight,
    sink_logit,
    out_pool_weight,
    out_attn_weight,
):
    rows, width = tokens.shape
    nsp = nz * NY
    dim = width * ntp
    qn, kn, pn = query_weight.shape[1], key_weight.shape[1], pool_in_weight.shape[1]
    fan = out_pool_weight.shape[0] + out_attn_weight.shape[0]
    ocols = out_pool_weight.shape[1]
    hbm = pl.BlockSpec(memory_space=pl.ANY)
    vmem = pl.BlockSpec(memory_space=pltpu.VMEM)
    smem = pl.BlockSpec(memory_space=pltpu.SMEM)
    dma = pltpu.SemaphoreType.DMA
    bf16 = jnp.bfloat16
    per_owner = nsp // ntp
    return pl.pallas_call(
        functools.partial(layer_kernel, nz, ntp),
        out_shape=(
            jax.ShapeDtypeStruct((rows, width), bf16),
            jax.ShapeDtypeStruct((sink_logit.shape[0], rows), jnp.float32),
        ),
        in_specs=[hbm, vmem, hbm, hbm, hbm, hbm, vmem, smem, hbm, hbm],
        out_specs=(vmem, vmem),
        scratch_shapes=[
            pltpu.VMEM((ntp, rows, width), bf16),
            pltpu.VMEM((rows, dim), bf16),
            pltpu.VMEM((dim, qn + 2 * kn + pn), bf16),
            pltpu.VMEM((nsp, fan, ocols), bf16),
            pltpu.VMEM((rows, qn), bf16),
            pltpu.VMEM((rows + 2 * WINDOW, 2 * kn + pn), bf16),
            pltpu.VMEM((rows, fan), bf16),
            pltpu.VMEM((nsp, rows, ocols), bf16),
            pltpu.VMEM((ntp, per_owner, rows, ocols), bf16),
            pltpu.VMEM((rows, 128), jnp.float32),
            pltpu.VMEM((rows, 128), jnp.float32),
            pltpu.VMEM((nsp, rows, ocols), bf16),
            pltpu.VMEM((nsp, rows, ocols), bf16),
            dma((7,)),
            dma((2, 3, nsp, PIECES)),
            dma((2, nsp, PIECES)),
            dma((ntp,)),
            dma((ntp,)),
            dma((2, 2)),
            dma((2, 2)),
            dma((nsp,)),
            dma((ntp, per_owner)),
            dma((nsp,)),
            dma((nsp,)),
        ],
        compiler_params=pltpu.CompilerParams(
            collective_id=0, has_side_effects=True, vmem_limit_bytes=56 << 20
        ),
    )(
        tokens,
        norm_gain[None, :],
        query_weight,
        key_weight,
        value_weight,
        pool_in_weight,
        pool_mix_weight,
        sink_logit,
        out_pool_weight,
        out_attn_weight,
    )


def choose(mesh):
    nsp, ntp = mesh.shape["sp"], mesh.shape["tp"]

    def body(*args):
        columns = args[8].shape[1]
        fits = nsp % NY == 0 and nsp % ntp == 0 and columns % 128 == 0 and ntp % 2 == 0
        if fits and args[0].shape[0] // WINDOW >= 2:
            return fused(nsp // NY, ntp, *args)
        return local(*args)

    return body


def solution(mesh):
    return jax.shard_map(
        choose(mesh),
        mesh=mesh,
        in_specs=(
            P("sp", "tp"),
            P(),
            P("sp", "tp"),
            P("sp", "tp"),
            P("sp", "tp"),
            P("sp", "tp"),
            P("tp", None, None),
            P("tp"),
            P("tp", "sp"),
            P("tp", "sp"),
        ),
        out_specs=(P("sp", "tp"), P("tp", "sp")),
        check_vma=False,
    )
```

profile of v0, /device:TPU:24, one launch (start us, length us, event | category | flops | bytes accessed | tf_op | source)
XLA Modules:
  0.0 99.1 jit_solution(4426766326669799865)
XLA Ops:
  0.6 96.0 %shard_map.113 = (bf16[512,512]{1,0:T(8,128)(2,1)}, f32[8,512]{1,0:T(8,128)}) custom-call(bf16[512,512]{1,0:T(8,128)(2,1)} %tok_ref.1, f32[1,2048]{1,0:T(1,128)} %bitcast.1, bf16[256,512]{1,0:T(8,128)(2,1)} %qw_ref.1, bf16[256,128]{1,0:T(8,128)(2,1)} %kw_ref.1, bf16[256,128]{1,0:T(8,128)(2,1)} %vw_ref.1, bf16[256,256]{1,0:T(8,128)(2,1)} %pw_ref.1, ...), custom_call_target="tpu_custom_call" | custom-call | tf_op jit(solution)/shard_map/pallas_call | solution.py:732
  96.6 0.0 copy-start
  96.6 1.9 %copy.14 = bf16[512,512]{1,0:T(8,128)(2,1)} copy(bf16[512,512]{1,0:T(8,128)(2,1)} %get-tuple-element.4) | data formatting | bytes 1048576
  98.5 0.0 copy-done
  98.5 0.6 copy.15
Async XLA Ops:
  96.6 1.9 %copy-start = (f32[8,512]{1,0:T(8,128)S(1)}, f32[8,512]{1,0:T(8,128)}, u32[]{:S(2)}) copy-start(f32[8,512]{1,0:T(8,128)} %get-tuple-element.5) | copy-start | bytes 49156
where the time goes:
time: 99.3 us; the launch traced here: 99.1 us
  Pallas kernels  96 us (97%)
  local copies, waits for them, and re-layouts  2.48 us (2%)
    pallas_call x1, Pallas kernels, fused(): pl.pallas_call(functools.partial(layer_kernel, nz, ntp), out_shape=(jax.S...  96 us
    unnamed x4, local copies, waits for them, and re-layouts  2.48 us

commit v1 on v0

v1 whole, which is shorter than its diff:
```python
import functools
import math

import jax
import jax.numpy as jnp
from jax import lax
from jax.experimental import pallas as pl
from jax.experimental.pallas import tpu as pltpu
from jax.sharding import PartitionSpec as P

HD = 64
WINDOW = 128
GRID_W = 64


norm_eps = 1e-06
rope_base = 10000.0
pool_reach = 8
neg_fill = -1e30


def with_halo(cells, sides, width):
    for axis, dim in sides:
        count = lax.axis_size(axis)
        ends = count - 1
        head = lax.slice_in_dim(cells, 0, width, axis=dim)
        tail = lax.slice_in_dim(cells, cells.shape[dim] - width, cells.shape[dim], axis=dim)
        cells = jnp.concatenate(
            [
                lax.ppermute(tail, axis, [(i, (i + 1) % count) for i in range(ends)]),
                cells,
                lax.ppermute(head, axis, [((i + 1) % count, i) for i in range(ends)]),
            ],
            axis=dim,
        )
    return cells


def rope_tables(positions, head_dim):
    n_freq = head_dim // 4
    freqs = rope_base ** (-jnp.arange(n_freq, dtype=jnp.float32) / n_freq)
    rows = (positions // GRID_W).astype(jnp.float32)
    columns = (positions % GRID_W).astype(jnp.float32)
    row_angle = rows[:, None] * freqs[None, :]
    col_angle = columns[:, None] * freqs[None, :]
    return (jnp.cos(row_angle), jnp.sin(row_angle), jnp.cos(col_angle), jnp.sin(col_angle))


def rotate_half(values, cosine, sine):
    middle = values.shape[-1] // 2
    first = values[..., :middle]
    second = values[..., middle:]
    return jnp.concatenate([first * cosine - second * sine, second * cosine + first * sine], -1)


def rotate_heads(values, tables, head_dim):
    rows_count = values.shape[0]
    shaped = values.astype(jnp.float32).reshape(rows_count, -1, head_dim)
    cos_r, sin_r, cos_c, sin_c = [table[:, None, :] for table in tables]
    split = head_dim // 2
    turned = jnp.concatenate(
        [
            rotate_half(shaped[..., :split], cos_r, sin_r),
            rotate_half(shaped[..., split:], cos_c, sin_c),
        ],
        -1,
    )
    return turned.reshape(rows_count, -1).astype(jnp.bfloat16)


def pool_group(extended, own, positions, half_width, seq_total):
    rows_count = own.shape[0]
    summed = jnp.zeros(own.shape, jnp.float32)
    counted = jnp.zeros((rows_count,), jnp.float32)
    for shift_by in range(-pool_reach, pool_reach):
        source = positions + shift_by
        inside = (
            (shift_by >= -half_width)
            & (shift_by < half_width)
            & (source >= 0)
            & (source < seq_total)
        )
        window_rows = extended[pool_reach + shift_by : pool_reach + shift_by + rows_count].astype(
            jnp.float32
        )
        summed = summed + jnp.where(inside[:, None], window_rows, 0.0)
        counted = counted + inside.astype(jnp.float32)
    return (summed / counted[:, None] - own.astype(jnp.float32)).astype(jnp.bfloat16)


def attend_block(queries, keys, values, sink, query_pos, key_pos, seq_total):
    scores = jnp.einsum(
        "qhgd,khd->hgqk", queries, keys, preferred_element_type=jnp.float32
    ) * HD ** (-0.5)
    valid = (
        (jnp.abs(query_pos[:, None] - key_pos[None, :]) <= WINDOW)
        & (key_pos >= 0)[None, :]
        & (key_pos < seq_total)[None, :]
    )
    scores = jnp.where(valid, scores, neg_fill)
    row_top = jnp.maximum(jnp.max(scores, -1), sink[:, :, None])
    exps = jnp.exp(scores - row_top[..., None])
    row_total = jnp.sum(exps, -1) + jnp.exp(sink[:, :, None] - row_top)
    weights = (exps / row_total[..., None]).astype(jnp.bfloat16)
    attended = jnp.einsum("hgqk,khd->qhgd", weights, values, preferred_element_type=jnp.float32)
    return (attended.astype(jnp.bfloat16), row_top + jnp.log(row_total))


def fetch_outputs(out_pool_weight, out_attn_weight):
    return (
        lax.all_gather(out_pool_weight, "sp", axis=1, tiled=True),
        lax.all_gather(out_attn_weight, "sp", axis=1, tiled=True),
    )


def local(
    tokens,
    norm_gain,
    query_weight,
    key_weight,
    value_weight,
    pool_in_weight,
    pool_mix_weight,
    sink_logit,
    out_pool_weight,
    out_attn_weight,
):
    whole = lax.all_gather(tokens, "tp", axis=1, tiled=True)
    wide = whole.astype(jnp.float32)
    normed = (
        wide * lax.rsqrt(jnp.mean(wide * wide, -1, keepdims=True) + norm_eps) * norm_gain
    ).astype(jnp.bfloat16)
    tok_rows = normed.shape[0]
    seq_total = tok_rows * lax.axis_size("sp")
    offset = lax.axis_index("sp") * tok_rows
    weights_in = (query_weight, key_weight, value_weight, pool_in_weight)
    pieces = (
        lax.all_gather(weights_in[0], "sp", axis=0, tiled=True),
        lax.all_gather(weights_in[1], "sp", axis=0, tiled=True),
        lax.all_gather(weights_in[2], "sp", axis=0, tiled=True),
        lax.all_gather(weights_in[3], "sp", axis=0, tiled=True),
    )
    sums = tuple((jnp.dot(normed, piece, preferred_element_type=jnp.float32) for piece in pieces))
    query, key, value, pool_input = [total.astype(jnp.bfloat16) for total in sums]
    positions = offset + jnp.arange(tok_rows, dtype=jnp.int32)
    tables = rope_tables(positions, HD)
    rot_query = rotate_heads(query, tables, HD)
    rot_key = rotate_heads(key, tables, HD)
    key_width = rot_key.shape[1]
    pool_ext = with_halo(pool_input, (("sp", 0),), pool_reach)
    pair_ext = with_halo(jnp.concatenate([rot_key, value], 1), (("sp", 0),), WINDOW)
    key_ext = pair_ext[:, :key_width]
    value_ext = pair_ext[:, key_width:]
    half_width = jnp.left_shift(jnp.int32(1), lax.axis_index("tp"))
    pooled = pool_group(pool_ext, pool_input, positions, half_width, seq_total)
    pool_out = jnp.dot(pooled, pool_mix_weight[0], preferred_element_type=jnp.float32).astype(
        jnp.bfloat16
    )
    heads_local = rot_query.shape[1] // HD
    kv_local = key_width // HD
    grp = heads_local // kv_local
    query_heads = rot_query.reshape(tok_rows, kv_local, grp, HD)
    key_heads = key_ext.reshape(-1, kv_local, HD)
    value_heads = value_ext.reshape(-1, kv_local, HD)
    sink = sink_logit.reshape(kv_local, grp)
    block_rows = min(tok_rows, 256)
    attended_parts = []
    log_parts = []
    for block_index in range(tok_rows // block_rows):
        start = block_index * block_rows
        query_pos = offset + start + jnp.arange(block_rows, dtype=jnp.int32)
        key_pos = offset + start - WINDOW + jnp.arange(block_rows + 2 * WINDOW, dtype=jnp.int32)
        attended_block, log_block = attend_block(
            query_heads[start : start + block_rows],
            key_heads[start : start + block_rows + 2 * WINDOW],
            value_heads[start : start + block_rows + 2 * WINDOW],
            sink,
            query_pos,
            key_pos,
            seq_total,
        )
        attended_parts.append(attended_block.reshape(block_rows, heads_local * HD))
        log_parts.append(log_block.reshape(heads_local, block_rows))
    attended = jnp.concatenate(attended_parts, 0)
    log_weight = jnp.concatenate(log_parts, 1)
    out_pool_full, out_attn_full = fetch_outputs(out_pool_weight, out_attn_weight)
    term = jnp.dot(pool_out, out_pool_full, preferred_element_type=jnp.float32)
    term = term + jnp.dot(attended, out_attn_full, preferred_element_type=jnp.float32)
    mixed = lax.psum_scatter(term.astype(jnp.bfloat16), "tp", scatter_dimension=1, tiled=True)
    return (mixed, log_weight)


NY = 2
NX = 2
CORES = 2
HALVES = 2
MESH = pl.DeviceIdType.MESH


def layer_kernel(
    nz,
    ntp,
    tok_ref,
    gain_ref,
    qw_ref,
    kw_ref,
    vw_ref,
    pw_ref,
    mix_ref,
    sink_ref,
    ow_ref,
    aw_ref,
    mixed_ref,
    log_ref,
    xg,
    normed,
    wg,
    wo,
    qrot,
    ext,
    act,
    part,
    rs1,
    tot,
    fin,
    cos_ref,
    sin_ref,
    mixb,
    sink_own,
    sinkb,
    log_own,
    log_in,
    load_send,
    load_recv,
    w_send,
    w_recv,
    x_loc,
    x_send,
    x_recv,
    xr_send,
    m_send,
    m_recv,
    h_send,
    h_recv,
    r1_send,
    r1_recv,
    r2_send,
    r2_recv,
):
    sp, tp = lax.axis_index("sp"), lax.axis_index("tp")
    z, y = sp // NY, sp % NY
    x, c = tp // CORES, tp % CORES
    nsp = nz * NY
    block_of = z * NY + c
    group_of = x * CORES + y
    straight = c == y
    crossed = c != y
    rows, width = tok_ref.shape
    brow = qw_ref.shape[0]
    qn, kn, pn = qw_ref.shape[1], kw_ref.shape[1], pw_ref.shape[1]
    heads, kv_local = qn // HD, kn // HD
    grp = heads // kv_local
    gw = 2 * kn
    groups = wg.shape[0]
    pool_rows = ow_ref.shape[0]
    ohalf = wo.shape[3]
    seq_total = rows * nsp
    per_owner = nsp // ntp
    pieces = groups + HALVES

    def at(zz, yy, xx, cc):
        return (zz * NY + yy, xx * CORES + cc)

    def remote(src, dst, send, recv, target):
        return pltpu.make_async_remote_copy(
            src_ref=src,
            dst_ref=dst,
            send_sem=send,
            recv_sem=recv,
            device_id=target,
            device_id_type=MESH,
        )

    sibling = at(z, y, x, 1 - c)
    partner = at(z, 1 - y, x, 1 - c)

    def shard_rows(block):
        return pl.ds(pl.multiple_of(block * brow, brow), brow)

    def load_parts(p, block):
        if p == 0:
            return [
                (kw_ref, wg.at[0, shard_rows(block), pl.ds(0, kn)]),
                (vw_ref, wg.at[0, shard_rows(block), pl.ds(kn, kn)]),
            ]
        if p == 2:
            return [(pw_ref, wg.at[2, shard_rows(block)])]
        if p < groups:
            return [(qw_ref.at[:, pl.ds((p // 2) * gw, gw)], wg.at[p, shard_rows(block)])]
        h = p - groups
        cols = pl.ds(h * ohalf, ohalf)
        return [
            (ow_ref.at[:, cols], wo.at[block, h, pl.ds(0, pool_rows)]),
            (aw_ref.at[:, cols], wo.at[block, h, pl.ds(pool_rows, wo.shape[2] - pool_rows)]),
        ]

    def load_local(p):
        return [
            pltpu.make_async_copy(a, b, load_recv.at[p, k])
            for k, (a, b) in enumerate(load_parts(p, sp))
        ]

    def load_swap(p):
        return [
            remote(a, b, load_send.at[p, k], load_recv.at[p, k], partner)
            for k, (a, b) in enumerate(load_parts(p, sp))
        ]

    def load_wait(p):
        @pl.when(straight)
        def _():
            for copy in load_local(p):
                copy.wait()

        @pl.when(crossed)
        def _():
            for k, (_, b) in enumerate(load_parts(p, block_of)):
                remote(b, b, load_send.at[p, k], load_recv.at[p, k], partner).wait_recv()

    onward = (z + 1 < nz, z >= 1)
    behind = (z, nz - 1 - z)

    def w_copy(p, block, way):
        ref = wg.at[p, shard_rows(block)] if p < groups else wo.at[block, p - groups]
        target = (at(z + 1, y, x, c), at(z - 1, y, x, c), sibling)[way]
        return remote(ref, ref, w_send.at[way, p, block], w_recv.at[p, block], target)

    def issue(copy, done):
        if done:
            copy.wait_send()
        else:
            copy.start()

    def send_own(p, ways, done=False):
        for way in ways:
            if way == 2:
                issue(w_copy(p, block_of, 2), done)
            else:

                @pl.when(onward[way])
                def _():
                    issue(w_copy(p, block_of, way), done)

    def relay(d, p, done=False):
        for way in range(2):
            source = (z - d, z + d)[way]
            block = source * NY + c

            @pl.when((source >= 0) & (source < nz))
            def _():
                if not done:
                    w_copy(p, block, 2).wait_recv()

                @pl.when(onward[way])
                def _():
                    issue(w_copy(p, block, way), done)

                issue(w_copy(p, block, 2), done)

    def stage(low, high):
        for total in range(low, high):
            for d in range(min(total, nz - 1) + 1):
                p = total - d
                if p < groups:
                    if d == 0:
                        load_wait(p)
                        send_own(p, (0, 1, 2))
                    else:
                        relay(d, p)

    def gathered(p):
        for source in range(nz):
            w_copy(p, source * NY + (1 - c), 2).wait_recv()

    cut = rows // 4
    spans = (pl.ds(0, cut), pl.ds(cut, rows - cut))

    def token_copy(kind, r):
        target = (at(z, y, x, y), at(z, y, 1 - x, y), at(z, 1 - y, x, y))[kind]
        return remote(
            tok_ref.at[spans[r]], xg.at[tp, spans[r]], x_send.at[kind, r], x_recv.at[tp, r], target
        )

    token_local = pltpu.make_async_copy(tok_ref, xg.at[tp], x_loc)

    def token_relay(k, r):
        slot = ((1 - x) if r == 0 else x) * CORES + k
        target = at(z, 1 - y, x, c) if r == 0 else at(z, y, 1 - x, c)
        ref = xg.at[slot, spans[r]]
        return remote(ref, ref, xr_send.at[k], x_recv.at[slot, r], target)

    def token_wait(slot, r):
        ref = xg.at[slot, spans[r]]
        remote(ref, ref, xr_send.at[0], x_recv.at[slot, r], sibling).wait_recv()

    mix_local = pltpu.make_async_copy(mix_ref.at[0], mixb, m_recv.at[0])
    mix_swap = remote(mix_ref.at[0], mixb, m_send.at[0], m_recv.at[0], partner)
    sink_swap = remote(sink_own, sinkb, m_send.at[1], m_recv.at[1], partner)

    @pl.when(straight)
    def _():
        for p in range(groups):
            for copy in load_local(p):
                copy.start()
        token_local.start()

    for head in range(heads):
        sink_own[head : head + 1, :] = jnp.full((1, 128), sink_ref[head], jnp.float32)

    @pl.when(straight)
    def _():
        sinkb[...] = sink_own[...]

    barrier = pltpu.get_barrier_semaphore()
    met = jnp.int32(0)
    for flip in range(1, NY * NX * CORES):
        fy, fx, fc = flip // 4, (flip // 2) % 2, flip % 2
        pl.semaphore_signal(
            barrier,
            inc=1,
            device_id=at(
                z,
                1 - y if fy else y,
                1 - x if fx else x,
                1 - c if fc else c,
            ),
            device_id_type=MESH,
        )
        met = met + 1
    for ok, zz in ((onward[0], z + 1), (onward[1], z - 1)):
        met = met + CORES * ok.astype(jnp.int32)

        @pl.when(ok)
        def _():
            for cc in range(CORES):
                pl.semaphore_signal(
                    barrier, inc=1, device_id=at(zz, y, x, cc), device_id_type=MESH
                )

    pl.semaphore_wait(barrier, met)

    @pl.when(straight)
    def _():
        for kind in (1, 2):
            for r in range(2):
                token_copy(kind, r if kind == 1 else 1 - r).start()
        mix_local.start()
        for p in range(groups, pieces):
            for copy in load_local(p):
                copy.start()

    @pl.when(crossed)
    def _():
        for copy in load_swap(0):
            copy.start()
        token_copy(2, 1).start()
        for r in range(2):
            token_copy(1, r).start()
            token_copy(0, r).start()
        for p in range(1, groups):
            for copy in load_swap(p):
                copy.start()
        token_copy(2, 0).start()
        sink_swap.start()
        mix_swap.start()
        for p in range(groups, pieces):
            for copy in load_swap(p):
                copy.start()

    stage(0, 1)
    ext[...] = jnp.zeros_like(ext)

    half = HD // 4
    lane = lax.broadcasted_iota(jnp.int32, (rows, 128), 1)
    is_first = (lane % (2 * half)) < half
    position = block_of * rows + lax.broadcasted_iota(jnp.int32, (rows, 128), 0)
    place = jnp.where((lane % HD) < 2 * half, position // GRID_W, position % GRID_W)
    freqs = jnp.exp((lane % half).astype(jnp.float32) * (-math.log(rope_base) / half))
    angle = place.astype(jnp.float32) * freqs
    cos_ref[...] = jnp.cos(angle)
    sine = jnp.sin(angle)
    sin_ref[...] = jnp.where(is_first, -sine, sine)

    stage(1, 2)
    for k in range(CORES):
        for r, ok in ((0, straight), (1, crossed)):

            @pl.when(ok)
            def _():
                token_relay(k, r).wait_recv()
                token_relay(k, r).start()

    stage(2, nz)

    @pl.when(straight)
    def _():
        token_local.wait()
        for r in range(2):
            token_wait(x * CORES + (1 - c), r)
        for k in range(CORES):
            token_wait((1 - x) * CORES + k, 1)

    @pl.when(crossed)
    def _():
        for k in range(CORES):
            token_wait(x * CORES + k, 0)
            for r in range(2):
                token_wait((1 - x) * CORES + k, r)

    norm_rows = 64

    @pl.loop(0, rows // norm_rows)
    def _(i):
        take = pl.ds(pl.multiple_of(i * norm_rows, norm_rows), norm_rows)
        pieces_in = [xg[t, take, :].astype(jnp.float32) for t in range(ntp)]
        total = sum(jnp.sum(piece * piece, -1, keepdims=True) for piece in pieces_in)
        scale = lax.rsqrt(total / (width * ntp) + norm_eps)
        for t in range(ntp):
            cols = pl.ds(t * width, width)
            normed[take, cols] = (pieces_in[t] * scale * gain_ref[:, cols]).astype(jnp.bfloat16)

    def turn(values, factor):
        wide = values.astype(jnp.bfloat16).astype(jnp.float32)
        swapped = jnp.where(
            is_first, pltpu.roll(wide, 128 - half, 1), pltpu.roll(wide, half, 1)
        )
        return ((wide * cos_ref[...] + swapped * sin_ref[...]) * factor).astype(jnp.bfloat16)

    def project(g):
        return jnp.dot(normed[...], wg[g], preferred_element_type=jnp.float32)

    mid = pl.ds(WINDOW, rows)
    edge = 16
    has_next, has_prev = block_of + 1 < nsp, block_of >= 1
    next_at = at(z + c, y, x, 1 - c)
    prev_at = at(z + c - 1, y, x, 1 - c)

    def halo_copy(way, what):
        cols = pl.ds(0, gw) if what == 0 else pl.ds(gw, pn)
        count = WINDOW if what == 0 else edge
        if way == 0:
            src, dst = WINDOW + rows - count, WINDOW - count
        else:
            src, dst = WINDOW, WINDOW + rows
        return remote(
            ext.at[pl.ds(src, count), cols],
            ext.at[pl.ds(dst, count), cols],
            h_send.at[way, what],
            h_recv.at[way, what],
            next_at if way == 0 else prev_at,
        )

    def halo_send(what, done=False):
        for way, ok in ((0, has_next), (1, has_prev)):

            @pl.when(ok)
            def _():
                issue(halo_copy(way, what), done)

    def halo_wait(what, near):
        for way, ok in ((0, has_prev), (1, has_next)):
            inside_chip = c == 1 if way == 0 else c == 0

            @pl.when(ok & (inside_chip if near else jnp.logical_not(inside_chip)))
            def _():
                halo_copy(way, what).wait_recv()

    gathered(0)
    pair = project(0)
    for col in range(0, kn, 128):
        ext[mid, col : col + 128] = turn(pair[:, col : col + 128], 1.0)
    ext[mid, kn:gw] = pair[:, kn:].astype(jnp.bfloat16)
    halo_send(0)

    stage(nz, nz + 1)
    for p in range(groups, pieces):
        load_wait(p)
        send_own(p, (2,))
        for way in range(2):

            @pl.when(onward[way] & (behind[way] <= 1))
            def _():
                w_copy(p, block_of, way).start()

    span = 3 * WINDOW
    row_at = lax.broadcasted_iota(jnp.int32, (WINDOW, span), 0)
    key_at = lax.broadcasted_iota(jnp.int32, (WINDOW, span), 1)
    apart = key_at - row_at
    lane_at = lax.broadcasted_iota(jnp.int32, (WINDOW, 128), 1)
    half_width = jnp.left_shift(jnp.int32(1), group_of)
    n_blocks = rows // WINDOW

    def inside_of(i):
        first = block_of * rows + (i - 1) * WINDOW
        return (key_at + first >= 0) & (key_at + first < seq_total)

    def attend(kv, i):
        q_at = pl.ds(pl.multiple_of(i * WINDOW, WINDOW), WINDOW)
        window = pl.ds(pl.multiple_of(i * WINDOW, WINDOW), span)
        valid = inside_of(i) & (apart >= 0) & (apart <= 2 * WINDOW)
        logs = jnp.zeros((WINDOW, 128), jnp.float32)
        keys = ext[window, kv * HD : (kv + 1) * HD]
        values = ext[window, kn + kv * HD : kn + (kv + 1) * HD]
        outs = []
        for g in range(grp):
            head = kv * grp + g
            query = qrot[q_at, head * HD : (head + 1) * HD]
            score = lax.dot_general(
                query, keys, (((1,), (1,)), ((), ())), preferred_element_type=jnp.float32
            )
            score = jnp.where(valid, score, neg_fill)
            sink = sinkb[head : head + 1, 0:1]
            top = jnp.maximum(jnp.max(score, -1, keepdims=True), sink)
            exps = jnp.exp(score - top)
            total = jnp.sum(exps, -1, keepdims=True) + jnp.exp(sink - top)
            weights = (exps * (1.0 / total)).astype(jnp.bfloat16)
            outs.append(jnp.dot(weights, values, preferred_element_type=jnp.float32))
            logs = jnp.where(lane_at == g, top + jnp.log(total), logs)
        for g in range(0, grp, 2):
            col = pn + (kv * grp + g) * HD
            act[q_at, col : col + 2 * HD] = jnp.concatenate(outs[g : g + 2], 1).astype(
                jnp.bfloat16
            )
        log_own[kv * grp : (kv + 1) * grp, q_at] = logs.T[:grp, :]

    late = jnp.where(c == 0, 0, n_blocks - 1)
    early = n_blocks - 1 - late

    def attend_early(kv):
        @pl.loop(0, n_blocks - 1)
        def _(j):
            attend(kv, jnp.where(j < n_blocks - 2, j + 1, early))

    def queries(kv, g):
        both = project(g)
        for col in range(0, gw, 128):
            qrot[:, kv * gw + col : kv * gw + col + 128] = turn(
                both[:, col : col + 128], HD ** -0.5
            )

    @pl.when(crossed)
    def _():
        remote(sink_own, sinkb, m_send.at[1], m_recv.at[1], partner).wait_recv()

    gathered(1)
    queries(0, 1)
    halo_wait(0, True)
    attend_early(0)

    stage(nz + 1, nz + 2)
    gathered(2)
    ext[mid, gw : gw + pn] = project(2).astype(jnp.bfloat16)
    halo_send(1)
    for p in range(groups, pieces):
        for way in range(2):

            @pl.when(onward[way] & (behind[way] > 1))
            def _():
                w_copy(p, block_of, way).start()

    stage(nz + 2, nz + groups)
    gathered(3)
    queries(1, 3)
    attend_early(1)

    if nz > 1:
        for p in range(groups, pieces):
            relay(1, p)

    halo_wait(0, False)
    for kv in range(kv_local):
        attend(kv, late)
    log_swap = remote(log_own, log_in, m_send.at[2], m_recv.at[2], partner)

    @pl.when(crossed)
    def _():
        log_swap.start()

    for near in (True, False):
        halo_wait(1, near)

    @pl.when(straight)
    def _():
        mix_local.wait()

    @pl.when(crossed)
    def _():
        mix_swap.wait_recv()

    @pl.loop(0, n_blocks)
    def _(i):
        q_at = pl.ds(pl.multiple_of(i * WINDOW, WINDOW), WINDOW)
        window = pl.ds(pl.multiple_of(i * WINDOW, WINDOW), span)
        own_at = pl.ds(pl.multiple_of((i + 1) * WINDOW, WINDOW), WINDOW)
        band = inside_of(i) & (apart >= WINDOW - half_width) & (apart < WINDOW + half_width)
        band_f = band.astype(jnp.float32)
        counted = jnp.sum(band_f, -1, keepdims=True)
        summed = jnp.dot(
            band_f.astype(jnp.bfloat16),
            ext[window, gw : gw + pn],
            preferred_element_type=jnp.float32,
        )
        own_pool = ext[own_at, gw : gw + pn]
        pooled = (summed / counted - own_pool.astype(jnp.float32)).astype(jnp.bfloat16)
        act[q_at, 0:pn] = jnp.dot(
            pooled, mixb[...], preferred_element_type=jnp.float32
        ).astype(jnp.bfloat16)

    hrow = rows // 2

    def r1_copy(block, h, rh):
        take = pl.ds(rh * hrow, hrow)
        return remote(
            part.at[block, h, take],
            rs1.at[block, h, take],
            r1_send.at[block, h, rh],
            r1_recv.at[block, h, rh],
            at(z, 1 - y, x, c),
        )

    def r2_copy(block, h, rh):
        take = pl.ds(rh * hrow, hrow)
        owner = block // per_owner
        slot = block % per_owner
        return remote(
            tot.at[block, h, take],
            fin.at[x, slot, h, take],
            r2_send.at[block, h, rh],
            r2_recv.at[x, slot, h, rh],
            (sp, owner),
        )

    def each_block(d, body):
        @pl.loop(0, 2 if d == 0 else 4)
        def _(k):
            source = z + (2 * (k // 2) - 1) * d

            @pl.when((source >= 0) & (source < nz))
            def _():
                mine = k % 2 == 0
                body(source * NY + jnp.where(mine, c, 1 - c), mine)

    def compute(d, h):
        def body(block, mine):
            @pl.when(jnp.logical_not(mine))
            def _():
                w_copy(groups + h, block, 2).wait_recv()

            part[block, h] = jnp.dot(
                act[...], wo[block, h], preferred_element_type=jnp.float32
            ).astype(jnp.bfloat16)

            @pl.when(crossed)
            def _():
                for rh in range(2):
                    r1_copy(block, h, rh).start()

        each_block(d, body)

    def join(d, h):
        def body(block, mine):
            for rh in range(2):
                take = pl.ds(rh * hrow, hrow)
                r1_copy(block, h, rh).wait_recv()
                tot[block, h, take] = (
                    part[block, h, take].astype(jnp.float32)
                    + rs1[block, h, take].astype(jnp.float32)
                ).astype(jnp.bfloat16)

                @pl.when(block // per_owner != tp)
                def _():
                    r2_copy(block, h, rh).start()

        @pl.when(straight)
        def _():
            each_block(d, body)

    order = [(d, h) for d in range(nz) for h in range(HALVES)]
    for n, (d, h) in enumerate(order):
        if d >= 2:
            relay(d, groups + h)
        compute(d, h)
        if n >= 1:
            join(*order[n - 1])
    join(*order[-1])

    @pl.when(straight)
    def _():
        log_ref[...] = log_own[...]

    @pl.when(crossed)
    def _():
        log_swap.wait_recv()
        log_ref[...] = log_in[...]

    for slot in range(per_owner):
        block = tp * per_owner + slot
        for h in range(HALVES):
            for rh in range(2):
                take = pl.ds(rh * hrow, hrow)
                for ok, side in ((crossed, x), (x >= 0, 1 - x)):

                    @pl.when(ok)
                    def _():
                        ref = fin.at[side, slot, h, take]
                        remote(
                            ref, ref, r2_send.at[0, h, rh], r2_recv.at[side, slot, h, rh], sibling
                        ).wait_recv()

                cols = slice(slot * HALVES * ohalf + h * ohalf, slot * HALVES * ohalf + (h + 1) * ohalf)
                far = fin[1 - x, slot, h, take].astype(jnp.float32)

                @pl.when(straight)
                def _():
                    near = tot[block, h, take].astype(jnp.float32)
                    mixed_ref[take, cols] = (near + far).astype(jnp.bfloat16)

                @pl.when(crossed)
                def _():
                    near = fin[x, slot, h, take].astype(jnp.float32)
                    mixed_ref[take, cols] = (near + far).astype(jnp.bfloat16)

    for p in range(pieces):
        send_own(p, (0, 1, 2), done=True)
        for d in range(1, nz):
            relay(d, p, done=True)
    halo_send(0, done=True)
    halo_send(1, done=True)

    for r, ok in ((0, straight), (1, crossed)):

        @pl.when(ok)
        def _():
            for kind in range(3):
                if not (r == 0 and kind == 0):
                    for s in range(2):
                        token_copy(kind, s).wait_send()
            for k in range(CORES):
                token_relay(k, r).wait_send()

    @pl.when(crossed)
    def _():
        for p in range(pieces):
            for copy in load_swap(p):
                copy.wait_send()
        mix_swap.wait_send()
        sink_swap.wait_send()
        log_swap.wait_send()

    @pl.loop(0, nsp)
    def _(block):
        for h in range(HALVES):
            for rh in range(2):

                @pl.when(crossed)
                def _():
                    r1_copy(block, h, rh).wait_send()

                @pl.when(straight & (block // per_owner != tp))
                def _():
                    r2_copy(block, h, rh).wait_send()


def fused(
    nz,
    ntp,
    tokens,
    norm_gain,
    query_weight,
    key_weight,
    value_weight,
    pool_in_weight,
    pool_mix_weight,
    sink_logit,
    out_pool_weight,
    out_attn_weight,
):
    rows, width = tokens.shape
    nsp = nz * NY
    dim = width * ntp
    qn, kn, pn = query_weight.shape[1], key_weight.shape[1], pool_in_weight.shape[1]
    fan = out_pool_weight.shape[0] + out_attn_weight.shape[0]
    ohalf = out_pool_weight.shape[1] // HALVES
    heads = sink_logit.shape[0]
    gw = 2 * kn
    groups = (qn + 2 * kn + pn) // gw
    pieces = groups + HALVES
    hbm = pl.BlockSpec(memory_space=pl.ANY)
    vmem = pl.BlockSpec(memory_space=pltpu.VMEM)
    smem = pl.BlockSpec(memory_space=pltpu.SMEM)
    dma = pltpu.SemaphoreType.DMA
    bf16 = jnp.bfloat16
    f32 = jnp.float32
    per_owner = nsp // ntp
    return pl.pallas_call(
        functools.partial(layer_kernel, nz, ntp),
        out_shape=(
            jax.ShapeDtypeStruct((rows, width), bf16),
            jax.ShapeDtypeStruct((heads, rows), f32),
        ),
        in_specs=[hbm, vmem, hbm, hbm, hbm, hbm, hbm, smem, hbm, hbm],
        out_specs=(vmem, vmem),
        scratch_shapes=[
            pltpu.VMEM((ntp, rows, width), bf16),
            pltpu.VMEM((rows, dim), bf16),
            pltpu.VMEM((groups, dim, gw), bf16),
            pltpu.VMEM((nsp, HALVES, fan, ohalf), bf16),
            pltpu.VMEM((rows, qn), bf16),
            pltpu.VMEM((rows + 2 * WINDOW, gw + pn), bf16),
            pltpu.VMEM((rows, fan), bf16),
            pltpu.VMEM((nsp, HALVES, rows, ohalf), bf16),
            pltpu.VMEM((nsp, HALVES, rows, ohalf), bf16),
            pltpu.VMEM((nsp, HALVES, rows, ohalf), bf16),
            pltpu.VMEM((NX, per_owner, HALVES, rows, ohalf), bf16),
            pltpu.VMEM((rows, 128), f32),
            pltpu.VMEM((rows, 128), f32),
            pltpu.VMEM((pn, pn), bf16),
            pltpu.VMEM((heads, 128), f32),
            pltpu.VMEM((heads, 128), f32),
            pltpu.VMEM((heads, rows), f32),
            pltpu.VMEM((heads, rows), f32),
            dma((pieces, 2)),
            dma((pieces, 2)),
            dma((3, pieces, nsp)),
            dma((pieces, nsp)),
            dma,
            dma((3, 2)),
            dma((ntp, 2)),
            dma((CORES,)),
            dma((3,)),
            dma((3,)),
            dma((2, 2)),
            dma((2, 2)),
            dma((nsp, HALVES, 2)),
            dma((nsp, HALVES, 2)),
            dma((nsp, HALVES, 2)),
            dma((NX, per_owner, HALVES, 2)),
        ],
        compiler_params=pltpu.CompilerParams(
            collective_id=0, has_side_effects=True, vmem_limit_bytes=56 << 20
        ),
    )(
        tokens,
        norm_gain[None, :],
        query_weight,
        key_weight,
        value_weight,
        pool_in_weight,
        pool_mix_weight,
        sink_logit,
        out_pool_weight,
        out_attn_weight,
    )


def choose(mesh):
    nsp, ntp = mesh.shape["sp"], mesh.shape["tp"]

    def body(*args):
        rows = args[0].shape[0]
        qn, kn, pn = args[2].shape[1], args[3].shape[1], args[5].shape[1]
        columns = args[8].shape[1]
        grid = nsp % NY == 0 and ntp == NX * CORES and nsp % ntp == 0
        cuts = columns % (HALVES * 128) == 0 and rows % (4 * WINDOW) == 0
        even = kn == 2 * HD and kn % 128 == 0 and qn == 4 * kn and pn == 2 * kn
        if grid and cuts and even:
            return fused(nsp // NY, ntp, *args)
        return local(*args)

    return body


def solution(mesh):
    return jax.shard_map(
        choose(mesh),
        mesh=mesh,
        in_specs=(
            P("sp", "tp"),
            P(),
            P("sp", "tp"),
            P("sp", "tp"),
            P("sp", "tp"),
            P("sp", "tp"),
            P("tp", None, None),
            P("tp"),
            P("tp", "sp"),
            P("tp", "sp"),
        ),
        out_specs=(P("sp", "tp"), P("tp", "sp")),
        check_vma=False,
    )
```

time: 99.3 us -> 97.7 us (0.984)
  the two profiles are of different devices: /device:TPU:24 before, /device:TPU:0 now
where the time goes in v1:
time: 97.7 us; the launch traced here: 97.5 us
  Pallas kernels  94.3 us (97%)
  local copies, waits for them, and re-layouts  2.48 us (3%)
    pallas_call x1, Pallas kernels, fused(): pl.pallas_call(functools.partial(layer_kernel, nz, ntp), out_shape=(jax.S...  94.3 us
    unnamed x4, local copies, waits for them, and re-layouts  2.48 us

profile of v1, /device:TPU:0, one launch (start us, length us, event | category | flops | bytes accessed | tf_op | source)
XLA Modules:
  0.0 97.5 jit_solution(830911408843717978)
XLA Ops:
  0.6 94.3 %shard_map.113 = (bf16[512,512]{1,0:T(8,128)(2,1)}, f32[8,512]{1,0:T(8,128)}) custom-call(bf16[512,512]{1,0:T(8,128)(2,1)} %tok_ref.1, f32[1,2048]{1,0:T(1,128)} %bitcast.1, bf16[256,512]{1,0:T(8,128)(2,1)} %qw_ref.1, bf16[256,128]{1,0:T(8,128)(2,1)} %kw_ref.1, bf16[256,128]{1,0:T(8,128)(2,1)} %vw_ref.1, bf16[256,256]{1,0:T(8,128)(2,1)} %pw_ref.1, ...), custom_call_target="tpu_custom_call" | custom-call | tf_op jit(solution)/shard_map/pallas_call | solution.py:905
  95.0 0.0 copy-start
  95.0 1.9 %copy.14 = bf16[512,512]{1,0:T(8,128)(2,1)} copy(bf16[512,512]{1,0:T(8,128)(2,1)} %get-tuple-element.4) | data formatting | bytes 1048576
  96.9 0.0 copy-done
  96.9 0.6 copy.15
Async XLA Ops:
  95.0 1.9 %copy-start = (f32[8,512]{1,0:T(8,128)S(1)}, f32[8,512]{1,0:T(8,128)}, u32[]{:S(2)}) copy-start(f32[8,512]{1,0:T(8,128)} %get-tuple-element.5) | copy-start | bytes 49156

commit v2 on v1

--- a/solution.py
+++ b/solution.py
@@ -226,6 +226,8 @@
     cos_ref,
     sin_ref,
     mixb,
+    gain,
+    sinks,
     sink_own,
     sinkb,
     log_own,
@@ -234,10 +236,12 @@
     load_recv,
     w_send,
     w_recv,
+    s_recv,
+    o_recv,
     x_loc,
     x_send,
     x_recv,
-    xr_send,
+    g_sem,
     m_send,
     m_recv,
     h_send,
@@ -293,10 +297,10 @@
                 (kw_ref, wg.at[0, shard_rows(block), pl.ds(0, kn)]),
                 (vw_ref, wg.at[0, shard_rows(block), pl.ds(kn, kn)]),
             ]
-        if p == 2:
-            return [(pw_ref, wg.at[2, shard_rows(block)])]
+        if p == 1:
+            return [(pw_ref, wg.at[1, shard_rows(block)])]
         if p < groups:
-            return [(qw_ref.at[:, pl.ds((p // 2) * gw, gw)], wg.at[p, shard_rows(block)])]
+            return [(qw_ref.at[:, pl.ds((p - 2) * gw, gw)], wg.at[p, shard_rows(block)])]
         h = p - groups
         cols = pl.ds(h * ohalf, ohalf)
         return [
@@ -306,81 +310,92 @@
 
     def load_local(p):
         return [
-            pltpu.make_async_copy(a, b, load_recv.at[p, k])
-            for k, (a, b) in enumerate(load_parts(p, sp))
+            pltpu.make_async_copy(a, b, load_recv.at[p]) for a, b in load_parts(p, sp)
         ]
 
     def load_swap(p):
         return [
-            remote(a, b, load_send.at[p, k], load_recv.at[p, k], partner)
-            for k, (a, b) in enumerate(load_parts(p, sp))
+            remote(a, b, load_send.at[p // groups], load_recv.at[p], partner)
+            for a, b in load_parts(p, sp)
         ]
 
+    def piece_of(p, block):
+        return wg.at[p, shard_rows(block)] if p < groups else wo.at[block, p - groups]
+
+    def arrived(ref, sem):
+        remote(ref, ref, load_send.at[0], sem, sibling).wait_recv()
+
+    def departed(ref, sem):
+        remote(ref, ref, sem, load_recv.at[0], sibling).wait_send()
+
     def load_wait(p):
-        @pl.when(straight)
-        def _():
-            for copy in load_local(p):
-                copy.wait()
-
-        @pl.when(crossed)
-        def _():
-            for k, (_, b) in enumerate(load_parts(p, block_of)):
-                remote(b, b, load_send.at[p, k], load_recv.at[p, k], partner).wait_recv()
+        arrived(piece_of(p, block_of), load_recv.at[p])
 
     onward = (z + 1 < nz, z >= 1)
-    behind = (z, nz - 1 - z)
+    middle = onward[0] & onward[1]
+    outer = jnp.logical_not(middle)
 
     def w_copy(p, block, way):
-        ref = wg.at[p, shard_rows(block)] if p < groups else wo.at[block, p - groups]
+        ref = piece_of(p, block)
         target = (at(z + 1, y, x, c), at(z - 1, y, x, c), sibling)[way]
-        return remote(ref, ref, w_send.at[way, p, block], w_recv.at[p, block], target)
-
-    def issue(copy, done):
-        if done:
-            copy.wait_send()
+        if way < 2:
+            recv = w_recv.at[p, block // NY]
+        elif p < groups:
+            recv = s_recv.at[p]
         else:
-            copy.start()
-
-    def send_own(p, ways, done=False):
+            recv = o_recv.at[p - groups, block // NY]
+        return remote(ref, ref, w_send.at[way, p // groups], recv, target)
+
+    def send_own(p, ways):
         for way in ways:
             if way == 2:
-                issue(w_copy(p, block_of, 2), done)
+                w_copy(p, block_of, 2).start()
             else:
 
                 @pl.when(onward[way])
                 def _():
-                    issue(w_copy(p, block_of, way), done)
-
-    def relay(d, p, done=False):
+                    w_copy(p, block_of, way).start()
+
+    def relay(d, p):
         for way in range(2):
             source = (z - d, z + d)[way]
             block = source * NY + c
 
             @pl.when((source >= 0) & (source < nz))
             def _():
-                if not done:
-                    w_copy(p, block, 2).wait_recv()
+                w_copy(p, block, way).wait_recv()
 
                 @pl.when(onward[way])
                 def _():
-                    issue(w_copy(p, block, way), done)
-
-                issue(w_copy(p, block, 2), done)
-
-    def stage(low, high):
-        for total in range(low, high):
-            for d in range(min(total, nz - 1) + 1):
-                p = total - d
-                if p < groups:
-                    if d == 0:
-                        load_wait(p)
-                        send_own(p, (0, 1, 2))
-                    else:
+                    w_copy(p, block, way).start()
+
+                w_copy(p, block, 2).start()
+
+    def stage(low, high, ok=None):
+        if ok is not None:
+
+            @pl.when(ok)
+            def _():
+                stage(low, high)
+
+            return
+        for turn_at in range(low, high):
+            for p in range(groups):
+                for role, when in ((straight, max(p - 1, 0)), (crossed, max(2 * p - 1, 0))):
+                    if when == turn_at:
+
+                        @pl.when(role)
+                        def _():
+                            load_wait(p)
+                            send_own(p, (0, 1, 2))
+
+            for d in range(1, nz):
+                for p in range(groups):
+                    if turn_at == 2 * p + d:
                         relay(d, p)
 
     def gathered(p):
-        for source in range(nz):
-            w_copy(p, source * NY + (1 - c), 2).wait_recv()
+        arrived(wg.at[p, pl.ds(0, nz * brow)], s_recv.at[p])
 
     cut = rows // 4
     spans = (pl.ds(0, cut), pl.ds(cut, rows - cut))
@@ -388,7 +403,7 @@
     def token_copy(kind, r):
         target = (at(z, y, x, y), at(z, y, 1 - x, y), at(z, 1 - y, x, y))[kind]
         return remote(
-            tok_ref.at[spans[r]], xg.at[tp, spans[r]], x_send.at[kind, r], x_recv.at[tp, r], target
+            tok_ref.at[spans[r]], xg.at[tp, spans[r]], x_send.at[0], x_recv.at[tp, r], target
         )
 
     token_local = pltpu.make_async_copy(tok_ref, xg.at[tp], x_loc)
@@ -397,15 +412,19 @@
         slot = ((1 - x) if r == 0 else x) * CORES + k
         target = at(z, 1 - y, x, c) if r == 0 else at(z, y, 1 - x, c)
         ref = xg.at[slot, spans[r]]
-        return remote(ref, ref, xr_send.at[k], x_recv.at[slot, r], target)
+        return remote(ref, ref, x_send.at[1], x_recv.at[slot, r], target)
 
     def token_wait(slot, r):
-        ref = xg.at[slot, spans[r]]
-        remote(ref, ref, xr_send.at[0], x_recv.at[slot, r], sibling).wait_recv()
+        arrived(xg.at[slot, spans[r]], x_recv.at[slot, r])
 
     mix_local = pltpu.make_async_copy(mix_ref.at[0], mixb, m_recv.at[0])
     mix_swap = remote(mix_ref.at[0], mixb, m_send.at[0], m_recv.at[0], partner)
     sink_swap = remote(sink_own, sinkb, m_send.at[1], m_recv.at[1], partner)
+
+    gain_load = pltpu.make_async_copy(gain_ref, gain, g_sem.at[0])
+    sink_load = pltpu.make_async_copy(sink_ref, sinks, g_sem.at[1])
+    sink_load.start()
+    gain_load.start()
 
     @pl.when(straight)
     def _():
@@ -413,13 +432,6 @@
             for copy in load_local(p):
                 copy.start()
         token_local.start()
-
-    for head in range(heads):
-        sink_own[head : head + 1, :] = jnp.full((1, 128), sink_ref[head], jnp.float32)
-
-    @pl.when(straight)
-    def _():
-        sinkb[...] = sink_own[...]
 
     barrier = pltpu.get_barrier_semaphore()
     met = jnp.int32(0)
@@ -447,6 +459,15 @@
                     barrier, inc=1, device_id=at(zz, y, x, cc), device_id_type=MESH
                 )
 
+    ext[...] = jnp.zeros_like(ext)
+    sink_load.wait()
+    for head in range(heads):
+        sink_own[head : head + 1, :] = jnp.full((1, 128), sinks[head], jnp.float32)
+
+    @pl.when(straight)
+    def _():
+        sinkb[...] = sink_own[...]
+
     pl.semaphore_wait(barrier, met)
 
     @pl.when(straight)
@@ -461,13 +482,12 @@
 
     @pl.when(crossed)
     def _():
-        for copy in load_swap(0):
-            copy.start()
-        token_copy(2, 1).start()
         for r in range(2):
             token_copy(1, r).start()
             token_copy(0, r).start()
-        for p in range(1, groups):
+        for p in range(groups):
+            if p == 2:
+                token_copy(2, 1).start()
             for copy in load_swap(p):
                 copy.start()
         token_copy(2, 0).start()
@@ -478,7 +498,6 @@
                 copy.start()
 
     stage(0, 1)
-    ext[...] = jnp.zeros_like(ext)
 
     half = HD // 4
     lane = lax.broadcasted_iota(jnp.int32, (rows, 128), 1)
@@ -492,15 +511,27 @@
     sin_ref[...] = jnp.where(is_first, -sine, sine)
 
     stage(1, 2)
-    for k in range(CORES):
-        for r, ok in ((0, straight), (1, crossed)):
-
-            @pl.when(ok)
-            def _():
-                token_relay(k, r).wait_recv()
-                token_relay(k, r).start()
-
-    stage(2, nz)
+
+    @pl.when(straight)
+    def _():
+        for k in range(CORES):
+            token_relay(k, 0).wait_recv()
+            token_relay(k, 0).start()
+
+    @pl.when(crossed)
+    def _():
+        token_relay(c, 1).wait_recv()
+        token_relay(c, 1).start()
+
+    stage(2, 3)
+
+    @pl.when(crossed)
+    def _():
+        token_relay(1 - c, 1).wait_recv()
+        token_relay(1 - c, 1).start()
+
+    stage(3, nz)
+    stage(nz, nz + 2, middle)
 
     @pl.when(straight)
     def _():
@@ -517,6 +548,7 @@
             for r in range(2):
                 token_wait((1 - x) * CORES + k, r)
 
+    gain_load.wait()
     norm_rows = 64
 
     @pl.loop(0, rows // norm_rows)
@@ -527,19 +559,22 @@
         scale = lax.rsqrt(total / (width * ntp) + norm_eps)
         for t in range(ntp):
             cols = pl.ds(t * width, width)
-            normed[take, cols] = (pieces_in[t] * scale * gain_ref[:, cols]).astype(jnp.bfloat16)
-
-    def turn(values, factor):
+            normed[take, cols] = (pieces_in[t] * scale * gain[:, cols]).astype(jnp.bfloat16)
+
+    hrow = rows // 2
+    lane_first = (lax.broadcasted_iota(jnp.int32, (hrow, 128), 1) % (2 * half)) < half
+
+    def turn(values, low, factor):
         wide = values.astype(jnp.bfloat16).astype(jnp.float32)
         swapped = jnp.where(
-            is_first, pltpu.roll(wide, 128 - half, 1), pltpu.roll(wide, half, 1)
-        )
-        return ((wide * cos_ref[...] + swapped * sin_ref[...]) * factor).astype(jnp.bfloat16)
-
-    def project(g):
-        return jnp.dot(normed[...], wg[g], preferred_element_type=jnp.float32)
-
-    mid = pl.ds(WINDOW, rows)
+            lane_first, pltpu.roll(wide, 128 - half, 1), pltpu.roll(wide, half, 1)
+        )
+        take = pl.ds(low, hrow)
+        return ((wide * cos_ref[take] + swapped * sin_ref[take]) * factor).astype(jnp.bfloat16)
+
+    def project(g, low):
+        return jnp.dot(normed[pl.ds(low, hrow)], wg[g], preferred_element_type=jnp.float32)
+
     edge = 16
     has_next, has_prev = block_of + 1 < nsp, block_of >= 1
     next_at = at(z + c, y, x, 1 - c)
@@ -565,7 +600,10 @@
 
             @pl.when(ok)
             def _():
-                issue(halo_copy(way, what), done)
+                if done:
+                    halo_copy(way, what).wait_send()
+                else:
+                    halo_copy(way, what).start()
 
     def halo_wait(what, near):
         for way, ok in ((0, has_prev), (1, has_next)):
@@ -576,27 +614,31 @@
                 halo_copy(way, what).wait_recv()
 
     gathered(0)
-    pair = project(0)
-    for col in range(0, kn, 128):
-        ext[mid, col : col + 128] = turn(pair[:, col : col + 128], 1.0)
-    ext[mid, kn:gw] = pair[:, kn:].astype(jnp.bfloat16)
+    for low in range(0, rows, hrow):
+        pair = project(0, low)
+        into = pl.ds(WINDOW + low, hrow)
+        for col in range(0, kn, 128):
+            ext[into, col : col + 128] = turn(pair[:, col : col + 128], low, 1.0)
+        ext[into, kn:gw] = pair[:, kn:].astype(jnp.bfloat16)
     halo_send(0)
 
-    stage(nz, nz + 1)
+    stage(nz + 2, nz + 4, middle)
+    stage(nz, nz + 2, outer)
+    gathered(1)
+    for low in range(0, rows, hrow):
+        ext[pl.ds(WINDOW + low, hrow), gw : gw + pn] = project(1, low).astype(jnp.bfloat16)
+    halo_send(1)
+    stage(nz + 4, nz + 2 * groups, middle)
     for p in range(groups, pieces):
         load_wait(p)
-        send_own(p, (2,))
-        for way in range(2):
-
-            @pl.when(onward[way] & (behind[way] <= 1))
-            def _():
-                w_copy(p, block_of, way).start()
+        send_own(p, (0, 1, 2))
 
     span = 3 * WINDOW
     row_at = lax.broadcasted_iota(jnp.int32, (WINDOW, span), 0)
     key_at = lax.broadcasted_iota(jnp.int32, (WINDOW, span), 1)
     apart = key_at - row_at
-    lane_at = lax.broadcasted_iota(jnp.int32, (WINDOW, 128), 1)
+    key_down = lax.broadcasted_iota(jnp.int32, (WINDOW, WINDOW), 0)
+    query_over = lax.broadcasted_iota(jnp.int32, (WINDOW, WINDOW), 1)
     half_width = jnp.left_shift(jnp.int32(1), group_of)
     n_blocks = rows // WINDOW
 
@@ -607,98 +649,60 @@
     def attend(kv, i):
         q_at = pl.ds(pl.multiple_of(i * WINDOW, WINDOW), WINDOW)
         window = pl.ds(pl.multiple_of(i * WINDOW, WINDOW), span)
-        valid = inside_of(i) & (apart >= 0) & (apart <= 2 * WINDOW)
-        logs = jnp.zeros((WINDOW, 128), jnp.float32)
+        first = block_of * rows + (i - 1) * WINDOW
+        low = (key_down >= query_over) & (first >= 0)
+        high = (key_down <= query_over) & (first + 2 * WINDOW < seq_total)
         keys = ext[window, kv * HD : (kv + 1) * HD]
-        values = ext[window, kn + kv * HD : kn + (kv + 1) * HD]
-        outs = []
+        values = ext[window, kn + kv * HD : kn + (kv + 1) * HD].T
+        weights, shares = [], []
         for g in range(grp):
             head = kv * grp + g
             query = qrot[q_at, head * HD : (head + 1) * HD]
             score = lax.dot_general(
-                query, keys, (((1,), (1,)), ((), ())), preferred_element_type=jnp.float32
+                keys, query, (((1,), (1,)), ((), ())), preferred_element_type=jnp.float32
             )
-            score = jnp.where(valid, score, neg_fill)
-            sink = sinkb[head : head + 1, 0:1]
-            top = jnp.maximum(jnp.max(score, -1, keepdims=True), sink)
+            score = jnp.concatenate(
+                [
+                    jnp.where(low, score[:WINDOW], neg_fill),
+                    score[WINDOW : 2 * WINDOW],
+                    jnp.where(high, score[2 * WINDOW :], neg_fill),
+                ],
+                0,
+            )
+            sink = sinkb[head : head + 1, :]
+            top = jnp.maximum(jnp.max(score, 0, keepdims=True), sink)
             exps = jnp.exp(score - top)
-            total = jnp.sum(exps, -1, keepdims=True) + jnp.exp(sink - top)
-            weights = (exps * (1.0 / total)).astype(jnp.bfloat16)
-            outs.append(jnp.dot(weights, values, preferred_element_type=jnp.float32))
-            logs = jnp.where(lane_at == g, top + jnp.log(total), logs)
-        for g in range(0, grp, 2):
-            col = pn + (kv * grp + g) * HD
-            act[q_at, col : col + 2 * HD] = jnp.concatenate(outs[g : g + 2], 1).astype(
-                jnp.bfloat16
-            )
-        log_own[kv * grp : (kv + 1) * grp, q_at] = logs.T[:grp, :]
+            total = jnp.sum(exps, 0, keepdims=True) + jnp.exp(sink - top)
+            log_own[head : head + 1, q_at] = top + jnp.log(total)
+            weights.append(exps.astype(jnp.bfloat16))
+            shares.append(1.0 / total)
+        out = jnp.dot(values, jnp.concatenate(weights, 1), preferred_element_type=jnp.float32)
+        outs = [out[:, g * WINDOW : (g + 1) * WINDOW] * shares[g] for g in range(grp)]
+        col = pn + kv * grp * HD
+        act[q_at, col : col + grp * HD] = jnp.concatenate(outs, 0).T.astype(jnp.bfloat16)
 
     late = jnp.where(c == 0, 0, n_blocks - 1)
     early = n_blocks - 1 - late
 
     def attend_early(kv):
-        @pl.loop(0, n_blocks - 1)
-        def _(j):
-            attend(kv, jnp.where(j < n_blocks - 2, j + 1, early))
+        for i in range(1, n_blocks - 1):
+            attend(kv, i)
+        attend(kv, early)
 
     def queries(kv, g):
-        both = project(g)
-        for col in range(0, gw, 128):
-            qrot[:, kv * gw + col : kv * gw + col + 128] = turn(
-                both[:, col : col + 128], HD ** -0.5
-            )
+        for low in range(0, rows, hrow):
+            both = project(g, low)
+            for col in range(0, gw, 128):
+                at_col = kv * gw + col
+                qrot[pl.ds(low, hrow), at_col : at_col + 128] = turn(
+                    both[:, col : col + 128], low, HD ** -0.5
+                )
 
     @pl.when(crossed)
     def _():
         remote(sink_own, sinkb, m_send.at[1], m_recv.at[1], partner).wait_recv()
 
-    gathered(1)
-    queries(0, 1)
-    halo_wait(0, True)
-    attend_early(0)
-
-    stage(nz + 1, nz + 2)
-    gathered(2)
-    ext[mid, gw : gw + pn] = project(2).astype(jnp.bfloat16)
-    halo_send(1)
-    for p in range(groups, pieces):
-        for way in range(2):
-
-            @pl.when(onward[way] & (behind[way] > 1))
-            def _():
-                w_copy(p, block_of, way).start()
-
-    stage(nz + 2, nz + groups)
-    gathered(3)
-    queries(1, 3)
-    attend_early(1)
-
-    if nz > 1:
-        for p in range(groups, pieces):
-            relay(1, p)
-
-    halo_wait(0, False)
-    for kv in range(kv_local):
-        attend(kv, late)
-    log_swap = remote(log_own, log_in, m_send.at[2], m_recv.at[2], partner)
-
-    @pl.when(crossed)
-    def _():
-        log_swap.start()
-
-    for near in (True, False):
-        halo_wait(1, near)
-
-    @pl.when(straight)
-    def _():
-        mix_local.wait()
-
-    @pl.when(crossed)
-    def _():
-        mix_swap.wait_recv()
-
-    @pl.loop(0, n_blocks)
-    def _(i):
+    def pool(i):
         q_at = pl.ds(pl.multiple_of(i * WINDOW, WINDOW), WINDOW)
         window = pl.ds(pl.multiple_of(i * WINDOW, WINDOW), span)
         own_at = pl.ds(pl.multiple_of((i + 1) * WINDOW, WINDOW), WINDOW)
@@ -716,15 +720,48 @@
             pooled, mixb[...], preferred_element_type=jnp.float32
         ).astype(jnp.bfloat16)
 
-    hrow = rows // 2
+    halo_wait(1, True)
+
+    @pl.when(straight)
+    def _():
+        mix_local.wait()
+
+    @pl.when(crossed)
+    def _():
+        mix_swap.wait_recv()
+
+    for i in range(1, n_blocks - 1):
+        pool(i)
+    pool(early)
+
+    stage(nz + 2, nz + 4, outer)
+    gathered(2)
+    queries(0, 2)
+    halo_wait(0, True)
+    attend_early(0)
+    stage(nz + 4, nz + 2 * groups, outer)
+    halo_wait(0, False)
+    attend(0, late)
+    halo_wait(1, False)
+    pool(late)
+
+    gathered(3)
+    queries(1, 3)
+    attend_early(1)
+    attend(1, late)
+    log_swap = remote(log_own, log_in, m_send.at[2], m_recv.at[2], partner)
+
+    @pl.when(crossed)
+    def _():
+        log_swap.start()
 
     def r1_copy(block, h, rh):
         take = pl.ds(rh * hrow, hrow)
         return remote(
-            part.at[block, h, take],
-            rs1.at[block, h, take],
-            r1_send.at[block, h, rh],
-            r1_recv.at[block, h, rh],
+            part.at[h, block, take],
+            rs1.at[h, block, take],
+            r1_send.at[h],
+            r1_recv.at[h, block, rh],
             at(z, 1 - y, x, c),
         )
 
@@ -732,11 +769,12 @@
         take = pl.ds(rh * hrow, hrow)
         owner = block // per_owner
         slot = block % per_owner
+        side = jnp.where(owner // CORES == x, 0, 1)
         return remote(
-            tot.at[block, h, take],
-            fin.at[x, slot, h, take],
-            r2_send.at[block, h, rh],
-            r2_recv.at[x, slot, h, rh],
+            tot.at[h, block, take],
+            fin.at[side, h, slot, take],
+            r2_send.at[h],
+            r2_recv.at[side, h, slot, rh],
             (sp, owner),
         )
 
@@ -756,7 +794,7 @@
             def _():
                 w_copy(groups + h, block, 2).wait_recv()
 
-            part[block, h] = jnp.dot(
+            part[h, block] = jnp.dot(
                 act[...], wo[block, h], preferred_element_type=jnp.float32
             ).astype(jnp.bfloat16)
 
@@ -772,9 +810,9 @@
             for rh in range(2):
                 take = pl.ds(rh * hrow, hrow)
                 r1_copy(block, h, rh).wait_recv()
-                tot[block, h, take] = (
-                    part[block, h, take].astype(jnp.float32)
-                    + rs1[block, h, take].astype(jnp.float32)
+                tot[h, block, take] = (
+                    part[h, block, take].astype(jnp.float32)
+                    + rs1[h, block, take].astype(jnp.float32)
                 ).astype(jnp.bfloat16)
 
                 @pl.when(block // per_owner != tp)
@@ -785,10 +823,22 @@
         def _():
             each_block(d, body)
 
+    def pass_on(d, h, ok):
+        @pl.when(ok)
+        def _():
+            relay(d, groups + h)
+
+    for h in range(HALVES):
+        pass_on(1, h, middle)
     order = [(d, h) for d in range(nz) for h in range(HALVES)]
     for n, (d, h) in enumerate(order):
-        if d >= 2:
-            relay(d, groups + h)
+        if d >= 1:
+            pass_on(d, h, outer)
+        if d == 2:
+            if h == 0:
+                for far in range(2, nz):
+                    for e in range(HALVES):
+                        pass_on(far, e, middle)
         compute(d, h)
         if n >= 1:
             join(*order[n - 1])
@@ -806,69 +856,74 @@
     for slot in range(per_owner):
         block = tp * per_owner + slot
         for h in range(HALVES):
+            low = (slot * HALVES + h) * ohalf
             for rh in range(2):
                 take = pl.ds(rh * hrow, hrow)
-                for ok, side in ((crossed, x), (x >= 0, 1 - x)):
+                for ok, side in ((crossed, 0), (tp >= 0, 1)):
 
                     @pl.when(ok)
                     def _():
-                        ref = fin.at[side, slot, h, take]
+                        ref = fin.at[side, h, slot, take]
                         remote(
-                            ref, ref, r2_send.at[0, h, rh], r2_recv.at[side, slot, h, rh], sibling
+                            ref, ref, r2_send.at[h], r2_recv.at[side, h, slot, rh], sibling
                         ).wait_recv()
 
-                cols = slice(slot * HALVES * ohalf + h * ohalf, slot * HALVES * ohalf + (h + 1) * ohalf)
-                far = fin[1 - x, slot, h, take].astype(jnp.float32)
+                far = fin[1, h, slot, take].astype(jnp.float32)
 
                 @pl.when(straight)
                 def _():
-                    near = tot[block, h, take].astype(jnp.float32)
-                    mixed_ref[take, cols] = (near + far).astype(jnp.bfloat16)
+                    near = tot[h, block, take].astype(jnp.float32)
+                    mixed_ref[take, low : low + ohalf] = (near + far).astype(jnp.bfloat16)
 
                 @pl.when(crossed)
                 def _():
-                    near = fin[x, slot, h, take].astype(jnp.float32)
-                    mixed_ref[take, cols] = (near + far).astype(jnp.bfloat16)
-
-    for p in range(pieces):
-        send_own(p, (0, 1, 2), done=True)
-        for d in range(1, nz):
-            relay(d, p, done=True)
+                    near = fin[0, h, slot, take].astype(jnp.float32)
+                    mixed_ref[take, low : low + ohalf] = (near + far).astype(jnp.bfloat16)
+
+    def all_sent(way, count):
+        departed(wg.at[pl.ds(0, groups), pl.ds(0, count * brow)], w_send.at[way, 0])
+        departed(wo.at[pl.ds(0, count)], w_send.at[way, 1])
+
+    all_sent(2, nz)
+    for count in range(1, nz):
+        for way, passed in ((0, z + 1), (1, nz - z)):
+
+            @pl.when(onward[way] & (passed == count))
+            def _():
+                all_sent(way, count)
+
     halo_send(0, done=True)
     halo_send(1, done=True)
 
-    for r, ok in ((0, straight), (1, crossed)):
-
-        @pl.when(ok)
-        def _():
-            for kind in range(3):
-                if not (r == 0 and kind == 0):
-                    for s in range(2):
-                        token_copy(kind, s).wait_send()
-            for k in range(CORES):
-                token_relay(k, r).wait_send()
+    @pl.when(straight)
+    def _():
+        departed(xg.at[pl.ds(0, 2)], x_send.at[0])
+        departed(xg.at[pl.ds(0, CORES), spans[0]], x_send.at[1])
+        for h in range(HALVES):
+            departed(tot.at[h, pl.ds(0, nsp - per_owner)], r2_send.at[h])
 
     @pl.when(crossed)
     def _():
-        for p in range(pieces):
-            for copy in load_swap(p):
-                copy.wait_send()
+        departed(xg.at[pl.ds(0, 3)], x_send.at[0])
+        departed(xg.at[pl.ds(0, CORES), spans[1]], x_send.at[1])
+        departed(wg.at[pl.ds(0, groups), pl.ds(0, brow)], load_send.at[0])
+        departed(wo.at[0], load_send.at[1])
         mix_swap.wait_send()
         sink_swap.wait_send()
         log_swap.wait_send()
-
-    @pl.loop(0, nsp)
-    def _(block):
         for h in range(HALVES):
-            for rh in range(2):
-
-                @pl.when(crossed)
-                def _():
-                    r1_copy(block, h, rh).wait_send()
-
-                @pl.when(straight & (block // per_owner != tp))
-                def _():
-                    r2_copy(block, h, rh).wait_send()
+            departed(part.at[h], r1_send.at[h])
+
+
+def place_kernel(mixed_ref, log_ref, mixed_out, log_out, sems):
+    copies = [
+        pltpu.make_async_copy(mixed_ref, mixed_out, sems.at[0]),
+        pltpu.make_async_copy(log_ref, log_out, sems.at[1]),
+    ]
+    for copy in copies:
+        copy.start()
+    for copy in copies:
+        copy.wait()
 
 
 def fused(
@@ -897,18 +952,18 @@
     pieces = groups + HALVES
     hbm = pl.BlockSpec(memory_space=pl.ANY)
     vmem = pl.BlockSpec(memory_space=pltpu.VMEM)
-    smem = pl.BlockSpec(memory_space=pltpu.SMEM)
     dma = pltpu.SemaphoreType.DMA
     bf16 = jnp.bfloat16
     f32 = jnp.float32
     per_owner = nsp // ntp
-    return pl.pallas_call(
+    outs = (
+        jax.ShapeDtypeStruct((rows, width), bf16),
+        jax.ShapeDtypeStruct((heads, rows), f32),
+    )
+    mixed, logs = pl.pallas_call(
         functools.partial(layer_kernel, nz, ntp),
-        out_shape=(
-            jax.ShapeDtypeStruct((rows, width), bf16),
-            jax.ShapeDtypeStruct((heads, rows), f32),
-        ),
-        in_specs=[hbm, vmem, hbm, hbm, hbm, hbm, hbm, smem, hbm, hbm],
+        out_shape=outs,
+        in_specs=[hbm] * 10,
         out_specs=(vmem, vmem),
         scratch_shapes=[
             pltpu.VMEM((ntp, rows, width), bf16),
@@ -918,33 +973,37 @@
             pltpu.VMEM((rows, qn), bf16),
             pltpu.VMEM((rows + 2 * WINDOW, gw + pn), bf16),
             pltpu.VMEM((rows, fan), bf16),
-            pltpu.VMEM((nsp, HALVES, rows, ohalf), bf16),
-            pltpu.VMEM((nsp, HALVES, rows, ohalf), bf16),
-            pltpu.VMEM((nsp, HALVES, rows, ohalf), bf16),
-            pltpu.VMEM((NX, per_owner, HALVES, rows, ohalf), bf16),
+            pltpu.VMEM((HALVES, nsp, rows, ohalf), bf16),
+            pltpu.VMEM((HALVES, nsp, rows, ohalf), bf16),
+            pltpu.VMEM((HALVES, nsp, rows, ohalf), bf16),
+            pltpu.VMEM((2, HALVES, per_owner, rows, ohalf), bf16),
             pltpu.VMEM((rows, 128), f32),
             pltpu.VMEM((rows, 128), f32),
             pltpu.VMEM((pn, pn), bf16),
+            pltpu.VMEM((1, dim), f32),
+            pltpu.SMEM((heads,), f32),
             pltpu.VMEM((heads, 128), f32),
             pltpu.VMEM((heads, 128), f32),
             pltpu.VMEM((heads, rows), f32),
             pltpu.VMEM((heads, rows), f32),
-            dma((pieces, 2)),
-            dma((pieces, 2)),
-            dma((3, pieces, nsp)),
-            dma((pieces, nsp)),
+            dma((2,)),
+            dma((pieces,)),
+            dma((3, 2)),
+            dma((pieces, nz)),
+            dma((groups,)),
+            dma((HALVES, nz)),
             dma,
-            dma((3, 2)),
+            dma((2,)),
             dma((ntp, 2)),
-            dma((CORES,)),
+            dma((2,)),
             dma((3,)),
             dma((3,)),
             dma((2, 2)),
             dma((2, 2)),
-            dma((nsp, HALVES, 2)),
-            dma((nsp, HALVES, 2)),
-            dma((nsp, HALVES, 2)),
-            dma((NX, per_owner, HALVES, 2)),
+            dma((HALVES,)),
+            dma((HALVES, nsp, 2)),
+            dma((HALVES,)),
+            dma((2, HALVES, per_owner, 2)),
         ],
         compiler_params=pltpu.CompilerParams(
             collective_id=0, has_side_effects=True, vmem_limit_bytes=56 << 20
@@ -961,6 +1020,13 @@
         out_pool_weight,
         out_attn_weight,
     )
+    return pl.pallas_call(
+        place_kernel,
+        out_shape=outs,
+        in_specs=[vmem, vmem],
+        out_specs=(hbm, hbm),
+        scratch_shapes=[dma((2,))],
+    )(mixed, logs)
 
 
 def choose(mesh):

time: 97.7 us -> 83.4 us (0.85)
  Pallas kernels: 94.3 us -> 82.6 us
  local copies, waits for them, and re-layouts: 2.48 us -> 0 us
    pallas_call x1 -> x2, Pallas kernels: 94.3 us -> 82.6 us  [the longest x1 80.7 us: fused(): pl.pallas_call(functools.partial(layer_kernel, nz, ntp), out_shape=outs,...]
    unnamed x4 -> x0, local copies, waits for them, and re-layouts: 2.48 us -> none
where the time goes in v2:
time: 83.4 us; the launch traced here: 83.2 us
  Pallas kernels  82.6 us (99%)
    pallas_call x1, Pallas kernels, fused(): pl.pallas_call(functools.partial(layer_kernel, nz, ntp), out_shape=outs,...  80.7 us
    pallas_call x1, Pallas kernels, fused(): pl.pallas_call(place_kernel, out_shape=outs, in_specs=[vmem, vmem], out_s...  1.86 us

profile of v2, /device:TPU:0, one launch (start us, length us, event | category | flops | bytes accessed | tf_op | source)
XLA Modules:
  0.0 83.2 jit_solution(2287042332750860689)
XLA Ops:
  0.6 80.7 %shard_map.113 = (bf16[512,512]{1,0:T(8,128)(2,1)}, f32[8,512]{1,0:T(8,128)}) custom-call(bf16[512,512]{1,0:T(8,128)(2,1)} %tok_ref.1, f32[1,2048]{1,0:T(1,128)} %bitcast.1, bf16[256,512]{1,0:T(8,128)(2,1)} %qw_ref.1, bf16[256,128]{1,0:T(8,128)(2,1)} %kw_ref.1, bf16[256,128]{1,0:T(8,128)(2,1)} %vw_ref.1, bf16[256,256]{1,0:T(8,128)(2,1)} %pw_ref.1, ...), custom_call_target="tpu_custom_call" | custom-call | tf_op jit(solution)/shard_map/pallas_call | solution.py:963
  81.4 1.9 %shard_map.114 = (bf16[512,512]{1,0:T(8,128)(2,1)}, f32[8,512]{1,0:T(8,128)}) custom-call(bf16[512,512]{1,0:T(8,128)(2,1)} %get-tuple-element.4.mixed_ref, f32[8,512]{1,0:T(8,128)} %get-tuple-element.5.log_ref), custom_call_target="tpu_custom_call" | custom-call | tf_op jit(solution)/shard_map/pallas_call | solution.py:1023

commit v3 on v2

--- a/solution.py
+++ b/solution.py
@@ -381,7 +381,7 @@
             return
         for turn_at in range(low, high):
             for p in range(groups):
-                for role, when in ((straight, max(p - 1, 0)), (crossed, max(2 * p - 1, 0))):
+                for role, when in ((straight, max(p - 1, 0)), (crossed, p)):
                     if when == turn_at:
 
                         @pl.when(role)
@@ -486,10 +486,9 @@
             token_copy(1, r).start()
             token_copy(0, r).start()
         for p in range(groups):
-            if p == 2:
-                token_copy(2, 1).start()
             for copy in load_swap(p):
                 copy.start()
+        token_copy(2, 1).start()
         token_copy(2, 0).start()
         sink_swap.start()
         mix_swap.start()
@@ -523,14 +522,13 @@
         token_relay(c, 1).wait_recv()
         token_relay(c, 1).start()
 
-    stage(2, 3)
+    stage(2, nz)
 
     @pl.when(crossed)
     def _():
         token_relay(1 - c, 1).wait_recv()
         token_relay(1 - c, 1).start()
 
-    stage(3, nz)
     stage(nz, nz + 2, middle)
 
     @pl.when(straight)
@@ -629,10 +627,22 @@
         ext[pl.ds(WINDOW + low, hrow), gw : gw + pn] = project(1, low).astype(jnp.bfloat16)
     halo_send(1)
     stage(nz + 4, nz + 2 * groups, middle)
-    for p in range(groups, pieces):
-        load_wait(p)
-        send_own(p, (0, 1, 2))
-
+    behind = (z, nz - 1 - z)
+
+    def own_out(ok, wait, ways, crowded):
+        @pl.when(ok)
+        def _():
+            for p in range(groups, pieces):
+                if wait:
+                    load_wait(p)
+                    w_copy(p, block_of, 2).start()
+                for way in ways:
+
+                    @pl.when(onward[way] & ((behind[way] > 1) == crowded))
+                    def _():
+                        w_copy(p, block_of, way).start()
+
+    own_out(outer, True, (0, 1), False)
     span = 3 * WINDOW
     row_at = lax.broadcasted_iota(jnp.int32, (WINDOW, span), 0)
     key_at = lax.broadcasted_iota(jnp.int32, (WINDOW, span), 1)
@@ -738,22 +748,14 @@
     gathered(2)
     queries(0, 2)
     halo_wait(0, True)
+    own_out(middle, True, (0, 1), False)
     attend_early(0)
+    own_out(middle, False, (0, 1), True)
     stage(nz + 4, nz + 2 * groups, outer)
     halo_wait(0, False)
     attend(0, late)
     halo_wait(1, False)
     pool(late)
-
-    gathered(3)
-    queries(1, 3)
-    attend_early(1)
-    attend(1, late)
-    log_swap = remote(log_own, log_in, m_send.at[2], m_recv.at[2], partner)
-
-    @pl.when(crossed)
-    def _():
-        log_swap.start()
 
     def r1_copy(block, h, rh):
         take = pl.ds(rh * hrow, hrow)
@@ -774,39 +776,41 @@
             tot.at[h, block, take],
             fin.at[side, h, slot, take],
             r2_send.at[h],
-            r2_recv.at[side, h, slot, rh],
+            r2_recv.at[side],
             (sp, owner),
         )
 
-    def each_block(d, body):
-        @pl.loop(0, 2 if d == 0 else 4)
-        def _(k):
-            source = z + (2 * (k // 2) - 1) * d
+    def each_block(d, lead, body):
+        parity = y if lead == 0 else 1 - y
+        for way in range(1 if d == 0 else 2):
+            source = z + (2 * way - 1) * d
 
             @pl.when((source >= 0) & (source < nz))
             def _():
-                mine = k % 2 == 0
-                body(source * NY + jnp.where(mine, c, 1 - c), mine)
-
-    def compute(d, h):
-        def body(block, mine):
-            @pl.when(jnp.logical_not(mine))
-            def _():
-                w_copy(groups + h, block, 2).wait_recv()
-
-            part[h, block] = jnp.dot(
-                act[...], wo[block, h], preferred_element_type=jnp.float32
+                body(source * NY + parity)
+
+    def compute(d, h, lead, halves=(0, 1)):
+        def body(block):
+            if halves[0] == 0:
+
+                @pl.when(crossed if lead == 0 else straight)
+                def _():
+                    w_copy(groups + h, block, 2).wait_recv()
+
+            take = pl.ds(halves[0] * hrow, len(halves) * hrow)
+            part[h, block, take] = jnp.dot(
+                act[take], wo[block, h], preferred_element_type=jnp.float32
             ).astype(jnp.bfloat16)
 
             @pl.when(crossed)
             def _():
-                for rh in range(2):
+                for rh in halves:
                     r1_copy(block, h, rh).start()
 
-        each_block(d, body)
+        each_block(d, lead, body)
 
     def join(d, h):
-        def body(block, mine):
+        def body(block):
             for rh in range(2):
                 take = pl.ds(rh * hrow, hrow)
                 r1_copy(block, h, rh).wait_recv()
@@ -821,28 +825,59 @@
 
         @pl.when(straight)
         def _():
-            each_block(d, body)
+            for lead in range(2):
+                each_block(d, lead, body)
+
+    gathered(3)
+    queries(1, 3)
+    log_swap = remote(log_own, log_in, m_send.at[2], m_recv.at[2], partner)
+
+    for rh in range(2):
+        for i in range(rh * n_blocks // 2, (rh + 1) * n_blocks // 2):
+            attend(1, i)
+        for h in range(HALVES):
+            for lead in range(2):
+                compute(0, h, lead, (rh,))
+
+    @pl.when(crossed)
+    def _():
+        log_swap.start()
 
     def pass_on(d, h, ok):
         @pl.when(ok)
         def _():
             relay(d, groups + h)
 
+    order = [(d, h) for d in range(nz) for h in range(HALVES)]
+
+    def advance(n):
+        d, h = order[n]
+        compute(d, h, 0)
+        pass_on(d, h, outer & crossed)
+        if n + 1 < len(order):
+            pass_on(*order[n + 1], outer & straight)
+        compute(d, h, 1)
+
     for h in range(HALVES):
         pass_on(1, h, middle)
-    order = [(d, h) for d in range(nz) for h in range(HALVES)]
-    for n, (d, h) in enumerate(order):
-        if d >= 1:
-            pass_on(d, h, outer)
-        if d == 2:
-            if h == 0:
-                for far in range(2, nz):
-                    for e in range(HALVES):
-                        pass_on(far, e, middle)
-        compute(d, h)
-        if n >= 1:
-            join(*order[n - 1])
-    join(*order[-1])
+    joined = 0
+    for n in range(HALVES, len(order)):
+        if n == HALVES:
+            pass_on(*order[n], outer & straight)
+        advance(n)
+        if n == 2 * HALVES - 1:
+            join(*order[0])
+            for far in range(2, nz):
+                for h in range(HALVES):
+                    pass_on(far, h, middle)
+            join(*order[1])
+            joined = 2
+        elif n >= 2 * HALVES:
+            while joined < n:
+                join(*order[joined])
+                joined += 1
+    for n in range(joined, len(order)):
+        join(*order[n])
 
     @pl.when(straight)
     def _():
@@ -853,32 +888,26 @@
         log_swap.wait_recv()
         log_ref[...] = log_in[...]
 
+    arrived(fin.at[1], r2_recv.at[1])
+
+    @pl.when(crossed)
+    def _():
+        arrived(fin.at[0], r2_recv.at[0])
+
     for slot in range(per_owner):
-        block = tp * per_owner + slot
         for h in range(HALVES):
             low = (slot * HALVES + h) * ohalf
-            for rh in range(2):
-                take = pl.ds(rh * hrow, hrow)
-                for ok, side in ((crossed, 0), (tp >= 0, 1)):
-
-                    @pl.when(ok)
-                    def _():
-                        ref = fin.at[side, h, slot, take]
-                        remote(
-                            ref, ref, r2_send.at[h], r2_recv.at[side, h, slot, rh], sibling
-                        ).wait_recv()
-
-                far = fin[1, h, slot, take].astype(jnp.float32)
-
-                @pl.when(straight)
-                def _():
-                    near = tot[h, block, take].astype(jnp.float32)
-                    mixed_ref[take, low : low + ohalf] = (near + far).astype(jnp.bfloat16)
-
-                @pl.when(crossed)
-                def _():
-                    near = fin[0, h, slot, take].astype(jnp.float32)
-                    mixed_ref[take, low : low + ohalf] = (near + far).astype(jnp.bfloat16)
+            far = fin[1, h, slot].astype(jnp.float32)
+
+            @pl.when(straight)
+            def _():
+                near = tot[h, tp * per_owner + slot].astype(jnp.float32)
+                mixed_ref[:, low : low + ohalf] = (near + far).astype(jnp.bfloat16)
+
+            @pl.when(crossed)
+            def _():
+                near = fin[0, h, slot].astype(jnp.float32)
+                mixed_ref[:, low : low + ohalf] = (near + far).astype(jnp.bfloat16)
 
     def all_sent(way, count):
         departed(wg.at[pl.ds(0, groups), pl.ds(0, count * brow)], w_send.at[way, 0])
@@ -1003,7 +1032,7 @@
             dma((HALVES,)),
             dma((HALVES, nsp, 2)),
             dma((HALVES,)),
-            dma((2, HALVES, per_owner, 2)),
+            dma((2,)),
         ],
         compiler_params=pltpu.CompilerParams(
             collective_id=0, has_side_effects=True, vmem_limit_bytes=56 << 20

time: 83.4 us -> 80.4 us (0.964)
  Pallas kernels: 82.6 us -> 79.5 us
    pallas_call x1, Pallas kernels: 80.7 us -> 77.6 us  [fused(): pl.pallas_call(functools.partial(layer_kernel, nz, ntp), out_shape=outs,...]
where the time goes in v3:
time: 80.4 us; the launch traced here: 80.3 us
  Pallas kernels  79.5 us (99%)
    pallas_call x1, Pallas kernels, fused(): pl.pallas_call(functools.partial(layer_kernel, nz, ntp), out_shape=outs,...  77.6 us
    pallas_call x1, Pallas kernels, fused(): pl.pallas_call(place_kernel, out_shape=outs, in_specs=[vmem, vmem], out_s...  1.86 us

profile of v3, /device:TPU:0, one launch (start us, length us, event | category | flops | bytes accessed | tf_op | source)
XLA Modules:
  0.0 80.3 jit_solution(1295792156557666692)
XLA Ops:
  0.6 77.6 %shard_map.113 = (bf16[512,512]{1,0:T(8,128)(2,1)}, f32[8,512]{1,0:T(8,128)}) custom-call(bf16[512,512]{1,0:T(8,128)(2,1)} %tok_ref.1, f32[1,2048]{1,0:T(1,128)} %bitcast.1, bf16[256,512]{1,0:T(8,128)(2,1)} %qw_ref.1, bf16[256,128]{1,0:T(8,128)(2,1)} %kw_ref.1, bf16[256,128]{1,0:T(8,128)(2,1)} %vw_ref.1, bf16[256,256]{1,0:T(8,128)(2,1)} %pw_ref.1, ...), custom_call_target="tpu_custom_call" | custom-call | tf_op jit(solution)/shard_map/pallas_call | solution.py:992
  78.2 1.9 %shard_map.114 = (bf16[512,512]{1,0:T(8,128)(2,1)}, f32[8,512]{1,0:T(8,128)}) custom-call(bf16[512,512]{1,0:T(8,128)(2,1)} %get-tuple-element.4.mixed_ref, f32[8,512]{1,0:T(8,128)} %get-tuple-element.5.log_ref), custom_call_target="tpu_custom_call" | custom-call | tf_op jit(solution)/shard_map/pallas_call | solution.py:1052

commit v4 on v3

--- a/solution.py
+++ b/solution.py
@@ -757,27 +757,32 @@
     halo_wait(1, False)
     pool(late)
 
-    def r1_copy(block, h, rh):
+    x_first = ((0, HALVES - 1), (2, 0))
+
+    def side_of(block):
+        return block // per_owner // CORES
+
+    def r1_copy(block, h, rh, turned):
         take = pl.ds(rh * hrow, hrow)
         return remote(
             part.at[h, block, take],
             rs1.at[h, block, take],
-            r1_send.at[h],
+            r1_send.at[h, int(turned)],
             r1_recv.at[h, block, rh],
-            at(z, 1 - y, x, c),
+            at(z, y, 1 - x, c) if turned else at(z, 1 - y, x, c),
         )
 
-    def r2_copy(block, h, rh):
+    def r2_copy(block, h, rh, turned):
         take = pl.ds(rh * hrow, hrow)
         owner = block // per_owner
         slot = block % per_owner
-        side = jnp.where(owner // CORES == x, 0, 1)
+        side = jnp.where(straight if turned else side_of(block) == x, 0, 1)
         return remote(
             tot.at[h, block, take],
             fin.at[side, h, slot, take],
-            r2_send.at[h],
+            r2_send.at[h, int(turned)],
             r2_recv.at[side],
-            (sp, owner),
+            (z * NY + c, owner),
         )
 
     def each_block(d, lead, body):
@@ -802,31 +807,38 @@
                 act[take], wo[block, h], preferred_element_type=jnp.float32
             ).astype(jnp.bfloat16)
 
-            @pl.when(crossed)
+            turned = (d, h) in x_first
+
+            @pl.when(side_of(block) != x if turned else crossed)
             def _():
                 for rh in halves:
-                    r1_copy(block, h, rh).start()
+                    r1_copy(block, h, rh, turned).start()
 
         each_block(d, lead, body)
 
     def join(d, h):
-        def body(block):
+        turned = (d, h) in x_first
+
+        def meet(block):
             for rh in range(2):
                 take = pl.ds(rh * hrow, hrow)
-                r1_copy(block, h, rh).wait_recv()
+                r1_copy(block, h, rh, turned).wait_recv()
                 tot[h, block, take] = (
                     part[h, block, take].astype(jnp.float32)
                     + rs1[h, block, take].astype(jnp.float32)
                 ).astype(jnp.bfloat16)
 
-                @pl.when(block // per_owner != tp)
+                @pl.when(crossed | (block // per_owner != tp))
                 def _():
-                    r2_copy(block, h, rh).start()
-
-        @pl.when(straight)
-        def _():
-            for lead in range(2):
-                each_block(d, lead, body)
+                    r2_copy(block, h, rh, turned).start()
+
+        def body(block):
+            @pl.when(side_of(block) == x if turned else straight)
+            def _():
+                meet(block)
+
+        for lead in range(2):
+            each_block(d, lead, body)
 
     gathered(3)
     queries(1, 3)
@@ -860,7 +872,6 @@
 
     for h in range(HALVES):
         pass_on(1, h, middle)
-    joined = 0
     for n in range(HALVES, len(order)):
         if n == HALVES:
             pass_on(*order[n], outer & straight)
@@ -870,14 +881,10 @@
             for far in range(2, nz):
                 for h in range(HALVES):
                     pass_on(far, h, middle)
-            join(*order[1])
-            joined = 2
-        elif n >= 2 * HALVES:
-            while joined < n:
-                join(*order[joined])
-                joined += 1
-    for n in range(joined, len(order)):
-        join(*order[n])
+        for ready in {4: (1, 2, 3), 6: (4, 5)}.get(n, ()):
+            join(*order[ready])
+    for ready in (6, 7):
+        join(*order[ready])
 
     @pl.when(straight)
     def _():
@@ -928,8 +935,6 @@
     def _():
         departed(xg.at[pl.ds(0, 2)], x_send.at[0])
         departed(xg.at[pl.ds(0, CORES), spans[0]], x_send.at[1])
-        for h in range(HALVES):
-            departed(tot.at[h, pl.ds(0, nsp - per_owner)], r2_send.at[h])
 
     @pl.when(crossed)
     def _():
@@ -940,8 +945,23 @@
         mix_swap.wait_send()
         sink_swap.wait_send()
         log_swap.wait_send()
-        for h in range(HALVES):
-            departed(part.at[h], r1_send.at[h])
+
+    for d, h in x_first:
+        across = z if d == 0 else (z + d) % nz
+        owner = across * NY // per_owner
+        facing = owner // CORES == x
+        plain = nsp - NY
+
+        def gone(ok, source, count, sem):
+            @pl.when(ok)
+            def _():
+                departed(source.at[h, pl.ds(0, count)], sem)
+
+        gone(jnp.logical_not(facing), part, NY, r1_send.at[h, 1])
+        gone(facing & (crossed | (owner != tp)), tot, NY, r2_send.at[h, 1])
+        gone(crossed, part, plain, r1_send.at[h, 0])
+        gone(straight & (owner == tp), tot, plain, r2_send.at[h, 0])
+        gone(straight & (owner != tp), tot, plain - per_owner, r2_send.at[h, 0])
 
 
 def place_kernel(mixed_ref, log_ref, mixed_out, log_out, sems):
@@ -1029,9 +1049,9 @@
             dma((3,)),
             dma((2, 2)),
             dma((2, 2)),
-            dma((HALVES,)),
+            dma((HALVES, 2)),
             dma((HALVES, nsp, 2)),
-            dma((HALVES,)),
+            dma((HALVES, 2)),
             dma((2,)),
         ],
         compiler_params=pltpu.CompilerParams(
@@ -1065,7 +1085,7 @@
         rows = args[0].shape[0]
         qn, kn, pn = args[2].shape[1], args[3].shape[1], args[5].shape[1]
         columns = args[8].shape[1]
-        grid = nsp % NY == 0 and ntp == NX * CORES and nsp % ntp == 0
+        grid = nsp == 4 * NY and ntp == NX * CORES and nsp == NY * ntp
         cuts = columns % (HALVES * 128) == 0 and rows % (4 * WINDOW) == 0
         even = kn == 2 * HD and kn % 128 == 0 and qn == 4 * kn and pn == 2 * kn
         if grid and cuts and even:

time: 80.4 us -> 80.3 us (level)
  no operation moved by 1% of the time
where the time goes in v4:
time: 80.3 us; the launch traced here: 80.2 us
  Pallas kernels  79.4 us (99%)
    pallas_call x1, Pallas kernels, fused(): pl.pallas_call(functools.partial(layer_kernel, nz, ntp), out_shape=outs,...  77.5 us
    pallas_call x1, Pallas kernels, fused(): pl.pallas_call(place_kernel, out_shape=outs, in_specs=[vmem, vmem], out_s...  1.86 us

profile of v4, /device:TPU:0, one launch (start us, length us, event | category | flops | bytes accessed | tf_op | source)
XLA Modules:
  0.0 80.2 jit_solution(12694712951984420852)
XLA Ops:
  0.6 77.5 %shard_map.113 = (bf16[512,512]{1,0:T(8,128)(2,1)}, f32[8,512]{1,0:T(8,128)}) custom-call(bf16[512,512]{1,0:T(8,128)(2,1)} %tok_ref.1, f32[1,2048]{1,0:T(1,128)} %bitcast.1, bf16[256,512]{1,0:T(8,128)(2,1)} %qw_ref.1, bf16[256,128]{1,0:T(8,128)(2,1)} %kw_ref.1, bf16[256,128]{1,0:T(8,128)(2,1)} %vw_ref.1, bf16[256,256]{1,0:T(8,128)(2,1)} %pw_ref.1, ...), custom_call_target="tpu_custom_call" | custom-call | tf_op jit(solution)/shard_map/pallas_call | solution.py:1012
  78.2 1.9 %shard_map.114 = (bf16[512,512]{1,0:T(8,128)(2,1)}, f32[8,512]{1,0:T(8,128)}) custom-call(bf16[512,512]{1,0:T(8,128)(2,1)} %get-tuple-element.4.mixed_ref, f32[8,512]{1,0:T(8,128)} %get-tuple-element.5.log_ref), custom_call_target="tpu_custom_call" | custom-call | tf_op jit(solution)/shard_map/pallas_call | solution.py:1072

commit v5 on v4

--- a/solution.py
+++ b/solution.py
@@ -547,7 +547,7 @@
                 token_wait((1 - x) * CORES + k, r)
 
     gain_load.wait()
-    norm_rows = 64
+    norm_rows = 128
 
     @pl.loop(0, rows // norm_rows)
     def _(i):

time: 80.3 us -> 80.6 us (level)
  no operation moved by 1% of the time
where the time goes in v5:
time: 80.6 us; the launch traced here: 80.4 us
  Pallas kernels  79.6 us (99%)
    pallas_call x1, Pallas kernels, fused(): pl.pallas_call(functools.partial(layer_kernel, nz, ntp), out_shape=outs,...  77.7 us
    pallas_call x1, Pallas kernels, fused(): pl.pallas_call(place_kernel, out_shape=outs, in_specs=[vmem, vmem], out_s...  1.86 us

profile of v5, /device:TPU:0, one launch (start us, length us, event | category | flops | bytes accessed | tf_op | source)
XLA Modules:
  0.0 80.4 jit_solution(1705708697800885597)
XLA Ops:
  0.6 77.7 %shard_map.113 = (bf16[512,512]{1,0:T(8,128)(2,1)}, f32[8,512]{1,0:T(8,128)}) custom-call(bf16[512,512]{1,0:T(8,128)(2,1)} %tok_ref.1, f32[1,2048]{1,0:T(1,128)} %bitcast.1, bf16[256,512]{1,0:T(8,128)(2,1)} %qw_ref.1, bf16[256,128]{1,0:T(8,128)(2,1)} %kw_ref.1, bf16[256,128]{1,0:T(8,128)(2,1)} %vw_ref.1, bf16[256,256]{1,0:T(8,128)(2,1)} %pw_ref.1, ...), custom_call_target="tpu_custom_call" | custom-call | tf_op jit(solution)/shard_map/pallas_call | solution.py:1012
  78.4 1.9 %shard_map.114 = (bf16[512,512]{1,0:T(8,128)(2,1)}, f32[8,512]{1,0:T(8,128)}) custom-call(bf16[512,512]{1,0:T(8,128)(2,1)} %get-tuple-element.4.mixed_ref, f32[8,512]{1,0:T(8,128)} %get-tuple-element.5.log_ref), custom_call_target="tpu_custom_call" | custom-call | tf_op jit(solution)/shard_map/pallas_call | solution.py:1072
